TPU v7x, 32 devices: a whole 2x2x4 slice. The times are simulated.
32 devices in a mesh: ep: 4 (over y, x), tp: 8 (over z, core).
Axes of the slice: x: 2, y: 2, z: 4, core: 2. Of those that a mesh axis runs over, the one named last changes fastest.
Arguments:
- tokens: bfloat16 [1024, 2048], P('ep'), may hold values from -6 to 6
- cotangent: bfloat16 [1024, 2048], P('ep'), may hold values from -6 to 6
- group_prob: float32 [1024], P('ep'), may hold values from 0.25 to 1
- expert_prob: float32 [1024, 2], P('ep'), may hold values from 0.1 to 1
- routing: int32 [1024, 2], P('ep'), may hold values from 0 to 3, all different within a row; in each aligned block of 256 rows (0 to 255, 256 to 511, ...) at most 192 rows name the same one
- gate_weight: bfloat16 [4, 2048, 4096], P('ep', None, 'tp'), may hold values from -0.125 to 0.125
- up_weight: bfloat16 [4, 2048, 4096], P('ep', None, 'tp'), may hold values from -0.125 to 0.125
- down_weight: bfloat16 [4, 4096, 2048], P('ep', 'tp'), may hold values from -1 to 1
Outputs:
- token_grad: bfloat16 [1024, 2048], P('ep')
- group_prob_grad: float32 [1024], P('ep')
- expert_prob_grad: float32 [1024, 2], P('ep')
- gate_weight_grad: bfloat16 [4, 2048, 4096], P('ep', None, 'tp')
- up_weight_grad: bfloat16 [4, 2048, 4096], P('ep', None, 'tp')
- down_weight_grad: bfloat16 [4, 4096, 2048], P('ep', 'tp')
- gate_row_norms: float32 [4, 2048], P('ep')
- up_row_norms: float32 [4, 2048], P('ep')
- down_row_norms: float32 [4, 4096], P('ep', 'tp')
Inputs may be any that keep to these rules, and one draw needn't show every extreme that they name: `routing`: each row names 2 different experts. In each aligned block of 256 rows no expert is named by more than 192 rows, and in every draw some expert is named by exactly 192 rows of some block.
All inputs are finite; a program needn't handle non-finite values.
Results may differ from a plain program's by a relative error of at most 0.0065.
Values may be sent and summed in bfloat16 or wider, within the bound.
A program may use at most 64 MiB of HBM per device.

v0:
```python
import jax
import jax.numpy as jnp
from jax import lax
from jax.sharding import PartitionSpec as P


def slot_targets(route_block, expert_count, capacity):
    flat = route_block.reshape(-1)
    names = jnp.arange(expert_count, dtype=jnp.int32)
    onehot = (flat[:, None] == names[None, :]).astype(jnp.int32)
    before = jnp.cumsum(onehot, axis=0) - onehot
    place = jnp.sum(before * onehot, axis=1)
    return flat * capacity + place


def local(tokens, cotangent, group_prob, expert_prob, routing, gate_weight, up_weight, down_weight):
    tok_count, model_width = tokens.shape
    top_count = routing.shape[1]
    expert_count = lax.axis_size("ep")
    capacity = 3 * tok_count * top_count // (2 * expert_count)
    slot_count = tok_count * top_count
    buffer_rows = expert_count * capacity
    target = slot_targets(routing, expert_count, capacity)
    weight = group_prob[:, None] * expert_prob
    flat_weight = weight.reshape(slot_count)
    owner = (
        jnp.full((buffer_rows,), slot_count, jnp.int32)
        .at[target]
        .set(jnp.arange(slot_count, dtype=jnp.int32))
    )
    filled = owner < slot_count
    safe_slot = jnp.minimum(owner, slot_count - 1)
    source = safe_slot // top_count
    send_in = jnp.where(filled[:, None], tokens[source], jnp.zeros((), jnp.bfloat16))
    send_in = send_in.reshape(expert_count, capacity, model_width)
    scaled = flat_weight[safe_slot][:, None] * cotangent[source].astype(jnp.float32)
    send_scaled = jnp.where(filled[:, None], scaled, 0.0).astype(jnp.bfloat16)
    send_scaled = send_scaled.reshape(expert_count, capacity, model_width)
    rows_in, rows_scaled = (
        lax.all_to_all(send_in, "ep", split_axis=0, concat_axis=0, tiled=True),
        lax.all_to_all(send_scaled, "ep", split_axis=0, concat_axis=0, tiled=True),
    )
    flat_in = rows_in.reshape(buffer_rows, model_width)
    flat_scaled = rows_scaled.reshape(buffer_rows, model_width)
    w_gate = gate_weight[0]
    w_up = up_weight[0]
    w_down = down_weight[0]
    hidden_total = gate_weight.shape[2] * lax.axis_size("tp")
    contract_last = (((1,), (1,)), ((), ()))
    contract_rows = (((0,), (0,)), ((), ()))
    pre_gate = jnp.dot(flat_in, w_gate, preferred_element_type=jnp.float32)
    pre_up = jnp.dot(flat_in, w_up, preferred_element_type=jnp.float32)
    sigma = jax.nn.sigmoid(pre_gate)
    activated = pre_gate * sigma
    derivative = sigma * (1.0 + pre_gate * (1.0 - sigma))
    hidden = (activated * pre_up).astype(jnp.bfloat16)
    hidden_grad = lax.dot_general(
        flat_scaled, w_down, contract_last, preferred_element_type=jnp.float32
    )
    score_part = jnp.sum(hidden.astype(jnp.float32) * hidden_grad, axis=1).reshape(
        expert_count, capacity
    )
    gate_pre = (hidden_grad * pre_up * derivative).astype(jnp.bfloat16)
    up_pre = (hidden_grad * activated).astype(jnp.bfloat16)
    down_sum = lax.dot_general(
        hidden, flat_scaled, contract_rows, preferred_element_type=jnp.float32
    )
    gate_sum = lax.dot_general(flat_in, gate_pre, contract_rows, preferred_element_type=jnp.float32)
    up_sum = lax.dot_general(flat_in, up_pre, contract_rows, preferred_element_type=jnp.float32)
    input_part = lax.dot_general(
        gate_pre, w_gate, contract_last, preferred_element_type=jnp.float32
    )
    input_part = input_part + lax.dot_general(
        up_pre, w_up, contract_last, preferred_element_type=jnp.float32
    )
    input_part = input_part.reshape(expert_count, capacity, model_width)
    norm_part = (
        jnp.stack([jnp.sum(gate_sum * gate_sum, axis=1), jnp.sum(up_sum * up_sum, axis=1)])
        / hidden_total
    )
    down_norms = jnp.sum(down_sum * down_sum, axis=1) / model_width
    share = lax.psum_scatter(input_part, "tp", scatter_dimension=2, tiled=True)
    scores, row_norms = lax.psum((score_part, norm_part), "tp")
    share = lax.all_to_all(
        share.astype(jnp.bfloat16), "ep", split_axis=0, concat_axis=0, tiled=True
    )
    returned_rows = lax.all_gather(share, "tp", axis=2, tiled=True)
    returned_scores = lax.all_to_all(scores, "ep", split_axis=0, concat_axis=0, tiled=True)
    per_slot = returned_rows.reshape(buffer_rows, model_width)[target]
    per_slot = per_slot.astype(jnp.float32).reshape(tok_count, top_count, model_width)
    token_grad = jnp.sum(per_slot, axis=1).astype(jnp.bfloat16)
    slot_score = returned_scores.reshape(buffer_rows)[target].reshape(tok_count, top_count) / weight
    expert_prob_grad = group_prob[:, None] * slot_score
    group_prob_grad = jnp.sum(expert_prob * slot_score, axis=1)
    return (
        token_grad,
        group_prob_grad,
        expert_prob_grad,
        gate_sum.astype(jnp.bfloat16)[None],
        up_sum.astype(jnp.bfloat16)[None],
        down_sum.astype(jnp.bfloat16)[None],
        row_norms[0][None],
        row_norms[1][None],
        down_norms[None],
    )


def solution(mesh):
    return jax.shard_map(
        local,
        mesh=mesh,
        in_specs=(
            P("ep", None),
            P("ep", None),
            P("ep"),
            P("ep", None),
            P("ep", None),
            P("ep", None, "tp"),
            P("ep", None, "tp"),
            P("ep", "tp", None),
        ),
        out_specs=(
            P("ep", None),
            P("ep"),
            P("ep", None),
            P("ep", None, "tp"),
            P("ep", None, "tp"),
            P("ep", "tp", None),
            P("ep", None),
            P("ep", None),
            P("ep", "tp"),
        ),
        check_vma=False,
    )
```

profile of v0, /device:TPU:0, one launch (start us, length us, event | category | flops | bytes accessed | tf_op | source)
XLA Modules:
  0.0 290.3 jit_solution(8094787610100634219)
XLA Ops:
  7.2 0.8 broadcast_multiply_fusion.3
  8.0 0.8 copy.20
  8.8 0.1 eq.29
  9.0 0.1 eq.25
  9.1 0.1 copy.19
  9.3 0.1 mul.82
  9.4 1.2 reduce-window.6
  10.7 0.2 slice_reduce_fusion
  10.9 0.2 reduce-window.9
  11.2 2.4 scatter_custom_fusion
  13.7 0.1 broadcast_in_dim.50
  13.8 8.5 %gather_fusion.2 = bf16[768,2048]{1,0:T(8,128)(2,1)} fusion(bf16[256,2048]{1,0:T(8,128)(2,1)} %param.8, s32[1024]{0:T(1024)S(1)} %get-tuple-element.45), kind=kCustom, calls=%fused_computation.2 | custom fusion | bytes 6294528 | tf_op jit(solution)/shard_map/gather | solution.py:34
  22.3 3.8 %broadcast_select_fusion = bf16[4,192,2048]{2,1,0:T(8,128)(2,1)} fusion(bf16[4,192,2048]{2,1,0:T(8,128)(2,1)} %bitcast.67, pred[4,192]{1,0:T(4,128)(4,1)S(1)} %broadcast_in_dim.50), kind=kLoop, calls=%fused_computation.13 | loop fusion | flops 1572864 | bytes 6292224 | tf_op jit(solution)/shard_map/jit(_where)/select_n | solution.py:34
  26.1 5.3 %all-to-all-start.1 = ((bf16[4,192,2048]{2,1,0:T(8,128)(2,1)}), bf16[4,192,2048]{2,1,0:T(8,128)(2,1)}, u32[]{:S(2)}, u32[]{:S(2)}) async-start(bf16[4,192,2048]{2,1,0:T(8,128)(2,1)} %broadcast_select_fusion), calls=%async_computation.1 | async-start | bytes 6291456 | tf_op jit(solution)/shard_map/all_to_all | solution.py:40
  31.4 0.1 copy.22
  31.6 0.1 broadcast_multiply_fusion.1
  31.7 0.1 reshape.126
  31.8 5.0 %gather_fusion = f32[768]{0:T(1024)S(1)} fusion(f32[512]{0:T(512)S(1)} %reshape.126, s32[1024]{0:T(1024)S(1)} %get-tuple-element.46), kind=kCustom, calls=%fused_computation | custom fusion | bytes 9216 | tf_op jit(solution)/shard_map/gather | solution.py:36
  36.9 4.2 %gather_fusion.1 = bf16[768,2048]{1,0:T(8,128)(2,1)} fusion(bf16[256,2048]{1,0:T(8,128)(2,1)S(1)} %copy-done.1, s32[1024]{0:T(1024)S(1)} %get-tuple-element.45), kind=kCustom, calls=%fused_computation.1 | custom fusion | bytes 6294528 | tf_op jit(solution)/shard_map/gather | solution.py:36
  41.2 4.4 %fusion.1 = bf16[4,192,2048]{2,1,0:T(8,128)(2,1)} fusion(bf16[4,192,2048]{2,1,0:T(8,128)(2,1)} %bitcast.66, f32[4,192]{1,0:T(4,128)S(1)} %mul.86, pred[4,192]{1,0:T(4,128)(4,1)S(1)} %broadcast_in_dim.50), kind=kLoop, calls=%fused_computation.8 | loop fusion | flops 6291456 | bytes 6295296 | tf_op jit(solution)/shard_map/convert_element_type | solution.py:37
  45.6 23.1 %all-to-all-done.1 = bf16[4,192,2048]{2,1,0:T(8,128)(2,1)} async-done(((bf16[4,192,2048]{2,1,0:T(8,128)(2,1)}), bf16[4,192,2048]{2,1,0:T(8,128)(2,1)}, u32[]{:S(2)}, u32[]{:S(2)}) %all-to-all-start.1) | async-done | bytes 3145760 | tf_op jit(solution)/shard_map/all_to_all | solution.py:40
  68.6 4.6 %all-to-all-start = ((bf16[4,192,2048]{2,1,0:T(8,128)(2,1)}), bf16[4,192,2048]{2,1,0:T(8,128)(2,1)}, u32[]{:S(2)}, u32[]{:S(2)}) async-start(bf16[4,192,2048]{2,1,0:T(8,128)(2,1)} %fusion.1), calls=%async_computation | async-start | bytes 6291456 | tf_op jit(solution)/shard_map/all_to_all | solution.py:41
  73.3 0.2 reduce-scatter.2.cloned.1.call-start
  73.5 5.0 %fusion.4 = f32[768,512]{0,1:T(8,128)} fusion(bf16[768,2048]{1,0:T(8,128)(2,1)} %bitcast.7, bf16[1,2048,512]{2,1,0:T(8,128)(2,1)S(1)} %copy-done), kind=kOutput, calls=%fused_computation.16 | convolution fusion | flops 1610612736 | bytes 6815744 | tf_op jit(solution)/shard_map/dot_general | solution.py:51
  78.5 4.9 %fusion.7 = f32[768,512]{0,1:T(8,128)} fusion(bf16[768,2048]{1,0:T(8,128)(2,1)} %bitcast.7, bf16[1,2048,512]{2,1,0:T(8,128)(2,1)S(1)} %copy-done.2), kind=kOutput, calls=%fused_computation.19 | convolution fusion | flops 1610612736 | bytes 6815744 | tf_op jit(solution)/shard_map/dot_general | solution.py:52
  83.4 25.7 %all-to-all-done = bf16[4,192,2048]{2,1,0:T(8,128)(2,1)} async-done(((bf16[4,192,2048]{2,1,0:T(8,128)(2,1)}), bf16[4,192,2048]{2,1,0:T(8,128)(2,1)}, u32[]{:S(2)}, u32[]{:S(2)}) %all-to-all-start) | async-done | bytes 3145760 | tf_op jit(solution)/shard_map/all_to_all | solution.py:41
  109.1 6.7 %multiply_reduce_fusion.3 = (f32[768]{0:T(1024)S(1)}, bf16[768,512]{0,1:T(8,128)(2,1)}, bf16[768,512]{0,1:T(8,128)(2,1)S(1)}, bf16[768,512]{0,1:T(8,128)(2,1)S(1)}) fusion(f32[768,512]{0,1:T(8,128)} %fusion.7, f32[768,512]{0,1:T(8,128)} %fusion.4, bf16[768,2048]{1,0:T(8,128)(2,1)} %bitcast.4, bf16[1,512,2048]{2,1,0:T(8,128)(2,1)} %param.15), kind=kOutput, calls=%fused_computation.26 | convolution fusion | flops 1617689856 | bytes 10750976 | tf_op jit(solution)/shard_map/dot_general | solution.py:57
  115.8 1.8 fusion.2
  117.7 4.5 %convolution_add_fusion = f32[768,2048]{1,0:T(8,128)} fusion(f32[768,2048]{1,0:T(8,128)S(1)} %fusion.2, bf16[768,512]{0,1:T(8,128)(2,1)S(1)} %get-tuple-element.38, bf16[1,2048,512]{2,1,0:T(8,128)(2,1)S(1)} %copy-done.3), kind=kOutput, calls=%fused_computation.12 | convolution fusion | flops 1612185600 | bytes 15466496 | tf_op jit(solution)/shard_map/dot_general | solution.py:73
  122.3 70.1 %reduce-scatter.2.cloned.1.call-done = f32[4,192,256]{2,1,0:T(8,128)} async-done(((f32[4,192,2048]{2,1,0:T(8,128)}), f32[4,192,256]{2,1,0:T(8,128)}) %reduce-scatter.2.cloned.1.call-update) | async-done | bytes 786448 | tf_op jit(solution)/shard_map/reduce_scatter | solution.py:82
  192.4 1.2 convert_element_type.52
  193.6 10.0 %all_to_all.24 = bf16[4,192,256]{2,1,0:T(8,128)(2,1)} all-to-all(bf16[4,192,256]{2,1,0:T(8,128)(2,1)S(1)} %convert_element_type.52), channel_id=1, replica_groups=mesh['ep'=4,'tp'=8] {'ep'}, dimensions={0} | all-to-all | bytes 786432 | tf_op jit(solution)/shard_map/all_to_all | solution.py:84
  203.7 5.3 %convert_bitcast_fusion.2 = (bf16[1,2048,512]{1,2,0:T(8,128)(2,1)}, f32[2048]{0:T(1024)S(1)}) fusion(bf16[768,512]{0,1:T(8,128)(2,1)} %copy-done.4, bf16[768,2048]{1,0:T(8,128)(2,1)} %bitcast.7), kind=kOutput, calls=%fused_computation.25 | convolution fusion | flops 1613756416 | bytes 6037504 | tf_op jit(solution)/shard_map/dot_general | solution.py:68
  209.0 5.2 %convert_bitcast_fusion.1 = (bf16[1,2048,512]{1,2,0:T(8,128)(2,1)}, f32[2048]{0:T(1024)S(1)}) fusion(bf16[768,512]{0,1:T(8,128)(2,1)S(1)} %get-tuple-element.38, bf16[768,2048]{1,0:T(8,128)(2,1)} %bitcast.7), kind=kOutput, calls=%fused_computation.24 | convolution fusion | flops 1613756416 | bytes 6037504 | tf_op jit(solution)/shard_map/dot_general | solution.py:69
  214.2 28.0 %all-reduce = (f32[4,1,192]{2,1,0:T(1,128)}, f32[2,2048]{1,0:T(2,128)S(1)}) all-reduce(f32[4,1,192]{2,1,0:T(1,128)S(1)} %all_to_all.18, f32[2,2048]{1,0:T(2,128)S(1)} %maximum_multiply_fusion), channel_id=1, replica_groups=mesh['ep'=4,'tp'=8] {'tp'}, use_global_device_ids=true, to_apply=%region_7.8 | all-reduce | flops 4864 | bytes 38912 | tf_op jit(solution)/shard_map/psum | solution.py:83
  242.2 3.5 %all-to-all-start.3 = ((f32[4,1,192]{2,1,0:T(1,128)}), f32[4,1,192]{2,1,0:T(1,128)S(1)}, u32[]{:S(2)}, u32[]{:S(2)}) async-start(f32[4,1,192]{2,1,0:T(1,128)} %get-tuple-element.27), calls=%async_computation.4 | async-start | bytes 8192 | tf_op jit(solution)/shard_map/all_to_all | solution.py:88
  245.7 0.6 fusion.20
  246.3 5.3 %multiply_reduce_fusion = (f32[512]{0:T(512)S(1)}, bf16[1,512,2048]{2,1,0:T(8,128)(2,1)}) fusion(bf16[768,512]{0,1:T(8,128)(2,1)} %get-tuple-element.30, bf16[768,2048]{1,0:T(8,128)(2,1)} %bitcast.4), kind=kOutput, calls=%fused_computation.9 | convolution fusion | flops 1613757952 | bytes 6031360 | tf_op jit(solution)/shard_map/dot_general | solution.py:65
  251.5 0.6 broadcast_multiply_fusion.2
  252.1 3.9 %copy.26 = bf16[1,2048,512]{2,1,0:T(8,128)(2,1)} copy(bf16[1,2048,512]{1,2,0:T(8,128)(2,1)} %get-tuple-element.34) | data formatting | bytes 4194304
  256.0 3.9 %copy.25 = bf16[1,2048,512]{2,1,0:T(8,128)(2,1)} copy(bf16[1,2048,512]{1,2,0:T(8,128)(2,1)} %get-tuple-element.36) | data formatting | bytes 4194304
  260.1 2.3 gather_fusion.4
  262.4 0.1 reshape.133
  262.5 0.8 broadcast_multiply_fusion
  263.3 0.7 copy.24
  263.9 7.5 %gather_fusion.3 = bf16[512,2048]{1,0:T(8,128)(2,1)} fusion(bf16[768,2048]{1,0:T(8,128)(2,1)} %bitcast.64, s32[1024]{0:T(1024)S(1)} %pad_clamp_fusion), kind=kCustom, calls=%fused_computation.3 | custom fusion | bytes 4196352 | tf_op jit(solution)/shard_map/gather | solution.py:89
  271.4 4.4 %gather.24 = bf16[256,2,2048]{2,1,0:T(2,128)(2,1)} reshape(bf16[512,2048]{1,0:T(8,128)(2,1)} %gather_fusion.3) | data formatting | bytes 4194304 | tf_op jit(solution)/shard_map/gather | solution.py:89
  275.8 7.7 %reduce_sum.70 = bf16[256,2048]{1,0:T(8,128)(2,1)} reduce(bf16[256,2,2048]{2,1,0:T(2,128)(2,1)} %gather.24, bf16[]{:T(256)} %constant.40.clone.1), dimensions={1}, to_apply=%region_5.6 | reduce | flops 524288 | bytes 3145730 | tf_op jit(solution)/shard_map/reduce_sum | solution.py:91
  (33 shorter events, 0.6 us)
Async XLA Ops:
  7.2 66.3 %copy-start = (bf16[1,2048,512]{2,1,0:T(8,128)(2,1)S(1)}, bf16[1,2048,512]{2,1,0:T(8,128)(2,1)}, u32[]{:S(2)}) copy-start(bf16[1,2048,512]{2,1,0:T(8,128)(2,1)} %param.13) | copy-start | bytes 6291460
  26.1 5.3 %copy-start.6 = (f32[256,2]{0,1:T(2,128)S(1)}, f32[256,2]{0,1:T(2,128)}, u32[]{:S(2)}) copy-start(f32[256,2]{0,1:T(2,128)} %param.11) | copy-start | bytes 6148
  26.1 5.5 %copy-start.5 = (f32[256]{0:T(256)S(1)}, f32[256]{0:T(256)}, u32[]{:S(2)}) copy-start(f32[256]{0:T(256)} %param.10) | copy-start | bytes 3076
  26.1 42.5 %all-to-all-start.1 = ((bf16[4,192,2048]{2,1,0:T(8,128)(2,1)}), bf16[4,192,2048]{2,1,0:T(8,128)(2,1)}, u32[]{:S(2)}, u32[]{:S(2)}) async-start(bf16[4,192,2048]{2,1,0:T(8,128)(2,1)} %broadcast_select_fusion), calls=%async_computation.1 | async-start | bytes 6291456 | tf_op jit(solution)/shard_map/all_to_all | solution.py:40
  31.8 5.1 %copy-start.1 = (bf16[256,2048]{1,0:T(8,128)(2,1)S(1)}, bf16[256,2048]{1,0:T(8,128)(2,1)}, u32[]{:S(2)}) copy-start(bf16[256,2048]{1,0:T(8,128)(2,1)} %param.9) | copy-start | bytes 3145732
  68.6 40.5 %all-to-all-start = ((bf16[4,192,2048]{2,1,0:T(8,128)(2,1)}), bf16[4,192,2048]{2,1,0:T(8,128)(2,1)}, u32[]{:S(2)}, u32[]{:S(2)}) async-start(bf16[4,192,2048]{2,1,0:T(8,128)(2,1)} %fusion.1), calls=%async_computation | async-start | bytes 6291456 | tf_op jit(solution)/shard_map/all_to_all | solution.py:41
  73.3 119.2 %reduce-scatter.2.cloned.1.call-start = ((), (), s32[]{:S(2)}) async-start(), calls=%async_computation.5 | async-start | bytes 7077888 | tf_op jit(solution)/shard_map/reduce_scatter | solution.py:82
  73.5 5.0 %copy-start.2 = (bf16[1,2048,512]{2,1,0:T(8,128)(2,1)S(1)}, bf16[1,2048,512]{2,1,0:T(8,128)(2,1)}, u32[]{:S(2)}) copy-start(bf16[1,2048,512]{2,1,0:T(8,128)(2,1)} %param.14) | copy-start | bytes 6291460
  115.8 1.9 copy-start.4
  115.8 1.9 copy-start.3
  122.3 141.6 %all-gather.2.cloned.1.call-start = ((), (), s32[]{:S(2)}) async-start(), calls=%async_computation.6 | async-start | bytes 3538944 | tf_op jit(solution)/shard_map/all_gather | solution.py:87
  242.2 17.8 %all-to-all-start.3 = ((f32[4,1,192]{2,1,0:T(1,128)}), f32[4,1,192]{2,1,0:T(1,128)S(1)}, u32[]{:S(2)}, u32[]{:S(2)}) async-start(f32[4,1,192]{2,1,0:T(1,128)} %get-tuple-element.27), calls=%async_computation.4 | async-start | bytes 8192 | tf_op jit(solution)/shard_map/all_to_all | solution.py:88
Sparse Core Ops, SparseCore 0:
  122.4 69.9 reduce-scatter.1
  203.7 37.3 all-gather.1
where the time goes:
time: 291 us; the launch traced here: 290 us
  waiting for transfers between devices  119 us (41%)
  local copies, waits for them, and re-layouts  45.9 us (16%)
  matrix products  38.7 us (13%)
  blocking collectives  38 us (13%)
  other arithmetic  20.9 us (7%)
  between operations  14.3 us (5%)
  starting transfers between devices  13.7 us (5%)
    reduce_scatter x1, waiting for transfers between devices, local(): share = lax.psum_scatter(input_part, 'tp', scatter_dimension=2, tiled=True)  70.1 us
    psum x1, blocking collectives, local(): scores, row_norms = lax.psum((score_part, norm_part), 'tp')  28 us
    all_to_all x1, waiting for transfers between devices, local(): lax.all_to_all(send_scaled, 'ep', split_axis=0, concat_axis=0, tiled=True)  25.7 us
    all_to_all x1, waiting for transfers between devices, local(): lax.all_to_all(send_in, 'ep', split_axis=0, concat_axis=0, tiled=True)  23.1 us
    gather x2, local copies, waits for them, and re-layouts, local(): per_slot = returned_rows.reshape(buffer_rows, model_width)[target]  11.9 us
    all_to_all x1, blocking collectives, local(): lax.all_to_all(share.astype(jnp.bfloat16), 'ep', split_axis=0, concat_axi...  9.97 us
    unnamed x19, local copies, waits for them, and re-layouts  9.48 us
    gather x1, local copies, waits for them, and re-layouts, local(): tokens[source]  8.5 us
  transfers between devices with their start and end apart: 5, of which 3 were waited for; matrix products, arithmetic and copies ran while one was open for 18% of the time, Pallas kernels for 0%

commit v1 on v0

v1 whole, which is shorter than its diff:
```python
import functools
import jax
import jax.numpy as jnp
from jax import lax
from jax.experimental import pallas as pl
from jax.experimental.pallas import tpu as pltpu
from jax.sharding import PartitionSpec as P

MESH = pl.DeviceIdType.MESH
CHUNKS = 4


def dispatch_kernel(n_ep, mine_ref, out_ref, local_sem, send_sem, recv_sem, fwd_send, fwd_recv):
    me = lax.axis_index("ep")
    t = lax.axis_index("tp")
    core = lax.rem(t, 2)
    partner = t + 1 - 2 * core
    width = mine_ref.shape[2] // CHUNKS
    barrier = pltpu.get_barrier_semaphore()
    for d in range(1, n_ep):
        pl.semaphore_signal(
            barrier, inc=1, device_id={"ep": lax.rem(me + d, n_ep)}, device_id_type=MESH
        )
    pl.semaphore_signal(barrier, inc=1, device_id={"tp": partner}, device_id_type=MESH)
    pl.semaphore_wait(barrier, n_ep)

    def cols(c):
        return pl.ds(c * width, width)

    def to_peer(d, c):
        dst = lax.rem(me + d, n_ep)
        return pltpu.make_async_remote_copy(
            src_ref=mine_ref.at[dst, :, cols(c)],
            dst_ref=out_ref.at[core, me, :, cols(c)],
            send_sem=send_sem.at[d, c],
            recv_sem=recv_sem.at[d, c],
            device_id={"ep": dst},
            device_id_type=MESH,
        )

    def from_peer(d, c):
        src = lax.rem(me - d + n_ep, n_ep)
        return pltpu.make_async_remote_copy(
            src_ref=mine_ref.at[me, :, cols(c)],
            dst_ref=out_ref.at[core, src, :, cols(c)],
            send_sem=send_sem.at[d, c],
            recv_sem=recv_sem.at[d, c],
            device_id={"ep": src},
            device_id_type=MESH,
        )

    def forward(d, c, side):
        src = lax.rem(me - d + n_ep, n_ep)
        source = mine_ref.at[me, :, cols(c)] if d == 0 else out_ref.at[side, src, :, cols(c)]
        return pltpu.make_async_remote_copy(
            src_ref=source,
            dst_ref=out_ref.at[side, src, :, cols(c)],
            send_sem=fwd_send.at[d, c],
            recv_sem=fwd_recv.at[d, c],
            device_id={"tp": partner},
            device_id_type=MESH,
        )

    order = sorted(range(1, n_ep), key=lambda d: abs(d - n_ep // 2))
    for c in range(CHUNKS):
        for d in order:
            to_peer(d, c).start()
    keep = pltpu.make_async_copy(mine_ref.at[me], out_ref.at[core, me], local_sem)
    keep.start()
    for c in range(CHUNKS):
        forward(0, c, core).start()
    for c in range(CHUNKS):
        for d in order:
            from_peer(d, c).wait_recv()
            forward(d, c, core).start()
    keep.wait()
    for c in range(CHUNKS):
        for d in order:
            to_peer(d, c).wait_send()
    for d in range(n_ep):
        for c in range(CHUNKS):
            forward(d, c, core).wait_send()
            forward(d, c, 1 - core).wait_recv()


def dispatch(mine, n_ep):
    return pl.pallas_call(
        functools.partial(dispatch_kernel, n_ep),
        out_shape=jax.ShapeDtypeStruct((2,) + mine.shape, mine.dtype),
        in_specs=[pl.BlockSpec(memory_space=pltpu.VMEM)],
        out_specs=pl.BlockSpec(memory_space=pl.ANY),
        scratch_shapes=[
            pltpu.SemaphoreType.DMA,
            pltpu.SemaphoreType.DMA((n_ep, CHUNKS)),
            pltpu.SemaphoreType.DMA((n_ep, CHUNKS)),
            pltpu.SemaphoreType.DMA((n_ep, CHUNKS)),
            pltpu.SemaphoreType.DMA((n_ep, CHUNKS)),
        ],
        compiler_params=pltpu.CompilerParams(collective_id=0, has_side_effects=True),
        name="dispatch",
    )(mine)


def sums_kernel(n_ep, n_tp, part_ref, norm_ref, score_ref, slots, total, send_sem, recv_sem, s_send, s_recv):
    me = lax.axis_index("ep")
    t = lax.axis_index("tp")
    barrier = pltpu.get_barrier_semaphore()
    for d in range(1, n_tp):
        pl.semaphore_signal(
            barrier, inc=1, device_id={"tp": lax.rem(t + d, n_tp)}, device_id_type=MESH
        )
    for d in range(1, n_ep):
        pl.semaphore_signal(
            barrier, inc=1, device_id={"ep": lax.rem(me + d, n_ep)}, device_id_type=MESH
        )
    pl.semaphore_wait(barrier, n_tp - 1 + n_ep - 1)

    def part_to(d):
        return pltpu.make_async_remote_copy(
            src_ref=part_ref,
            dst_ref=slots.at[t],
            send_sem=send_sem.at[d],
            recv_sem=recv_sem.at[d],
            device_id={"tp": lax.rem(t + d, n_tp)},
            device_id_type=MESH,
        )

    def part_from(d):
        src = lax.rem(t - d + n_tp, n_tp)
        return pltpu.make_async_remote_copy(
            src_ref=part_ref,
            dst_ref=slots.at[src],
            send_sem=send_sem.at[d],
            recv_sem=recv_sem.at[d],
            device_id={"tp": src},
            device_id_type=MESH,
        )

    for d in range(1, n_tp):
        part_to(d).start()
    slots[t] = part_ref[...]
    for d in range(1, n_tp):
        part_from(d).wait_recv()
    acc = slots[0]
    for i in range(1, n_tp):
        acc = acc + slots[i]
    total[...] = acc
    rows = 8 * n_ep

    def score_to(d):
        dst = lax.rem(me + d, n_ep)
        return pltpu.make_async_remote_copy(
            src_ref=total.at[pl.ds(pl.multiple_of(dst * 8, 8), 8)],
            dst_ref=score_ref.at[me],
            send_sem=s_send.at[d],
            recv_sem=s_recv.at[d],
            device_id={"ep": dst},
            device_id_type=MESH,
        )

    def score_from(d):
        src = lax.rem(me - d + n_ep, n_ep)
        return pltpu.make_async_remote_copy(
            src_ref=total.at[pl.ds(0, 8)],
            dst_ref=score_ref.at[src],
            send_sem=s_send.at[d],
            recv_sem=s_recv.at[d],
            device_id={"ep": src},
            device_id_type=MESH,
        )

    norm_ref[...] = acc[rows:]
    for d in range(1, n_tp):
        part_to(d).wait_send()
    for d in range(1, n_ep):
        score_to(d).start()
    score_ref[me] = total[pl.ds(pl.multiple_of(me * 8, 8), 8)]
    for d in range(1, n_ep):
        score_from(d).wait_recv()
    for d in range(1, n_ep):
        score_to(d).wait_send()


def small_sums(scores, norms, n_ep, n_tp):
    cap = scores.shape[1]
    width = norms.shape[1]
    padded = jnp.pad(scores, ((0, 0), (0, 1024 - cap))).reshape(n_ep * 8, 128)
    part = jnp.concatenate([padded, norms.reshape(2 * width // 128, 128)], axis=0)
    norm_out, score_out = pl.pallas_call(
        functools.partial(sums_kernel, n_ep, n_tp),
        out_shape=(
            jax.ShapeDtypeStruct((2 * width // 128, 128), jnp.float32),
            jax.ShapeDtypeStruct((n_ep, 8, 128), jnp.float32),
        ),
        in_specs=[pl.BlockSpec(memory_space=pltpu.VMEM)],
        out_specs=(
            pl.BlockSpec(memory_space=pltpu.VMEM),
            pl.BlockSpec(memory_space=pltpu.VMEM),
        ),
        scratch_shapes=[
            pltpu.VMEM((n_tp,) + part.shape, jnp.float32),
            pltpu.VMEM(part.shape, jnp.float32),
            pltpu.SemaphoreType.DMA((n_tp,)),
            pltpu.SemaphoreType.DMA((n_tp,)),
            pltpu.SemaphoreType.DMA((n_ep,)),
            pltpu.SemaphoreType.DMA((n_ep,)),
        ],
        compiler_params=pltpu.CompilerParams(collective_id=1, has_side_effects=True),
        cost_estimate=pl.CostEstimate(flops=0, bytes_accessed=20_000_000, transcendentals=0),
        name="small_sums",
    )(part)
    return score_out.reshape(n_ep, 1024)[:, :cap], norm_out.reshape(2, width)


def local(tokens, cotangent, group_prob, expert_prob, routing, gate_weight, up_weight, down_weight):
    tok_count, model_width = tokens.shape
    top_count = routing.shape[1]
    n_ep = lax.axis_size("ep")
    n_tp = lax.axis_size("tp")
    capacity = 3 * tok_count * top_count // (2 * n_ep)
    buffer_rows = n_ep * capacity
    core = lax.rem(lax.axis_index("tp"), 2)
    weight = group_prob[:, None] * expert_prob

    experts = jnp.arange(n_ep, dtype=jnp.int32)[:, None]
    picks = [routing[None, :, k] == experts for k in range(top_count)]
    named = functools.reduce(jnp.logical_or, picks)
    weight_of = sum(jnp.where(picks[k], weight[None, :, k], 0.0) for k in range(top_count))
    earlier = (
        lax.broadcasted_iota(jnp.int32, (tok_count, tok_count), 0)
        < lax.broadcasted_iota(jnp.int32, (tok_count, tok_count), 1)
    ).astype(jnp.bfloat16)
    before = jnp.dot(named.astype(jnp.bfloat16), earlier, preferred_element_type=jnp.float32)
    place = jnp.where(named, before.astype(jnp.int32), -1)
    filled = place[:, None, :] == lax.broadcasted_iota(jnp.int32, (n_ep, capacity, tok_count), 1)
    pick = filled.astype(jnp.bfloat16).reshape(buffer_rows, tok_count)
    slot_weight = jnp.sum(jnp.where(filled, weight_of[:, None, :], 0.0), axis=2).reshape(buffer_rows, 1)

    source = jnp.where(core == 0, tokens, cotangent)
    factor = jnp.where(core == 0, 1.0, slot_weight)
    mine = jnp.dot(pick, source, preferred_element_type=jnp.float32) * factor
    mine = mine.astype(jnp.bfloat16).reshape(n_ep, capacity, model_width)
    both = dispatch(mine, n_ep)
    flat_in = both[0].reshape(buffer_rows, model_width)
    flat_scaled = both[1].reshape(buffer_rows, model_width)

    w_gate = gate_weight[0]
    w_up = up_weight[0]
    w_down = down_weight[0]
    hidden_total = gate_weight.shape[2] * n_tp
    contract_last = (((1,), (1,)), ((), ()))
    contract_rows = (((0,), (0,)), ((), ()))
    pre_gate = jnp.dot(flat_in, w_gate, preferred_element_type=jnp.float32)
    pre_up = jnp.dot(flat_in, w_up, preferred_element_type=jnp.float32)
    sigma = jax.nn.sigmoid(pre_gate)
    activated = pre_gate * sigma
    derivative = sigma * (1.0 + pre_gate * (1.0 - sigma))
    hidden = (activated * pre_up).astype(jnp.bfloat16)
    hidden_grad = lax.dot_general(
        flat_scaled, w_down, contract_last, preferred_element_type=jnp.float32
    )
    score_part = jnp.sum(hidden.astype(jnp.float32) * hidden_grad, axis=1).reshape(n_ep, capacity)
    gate_pre = (hidden_grad * pre_up * derivative).astype(jnp.bfloat16)
    up_pre = (hidden_grad * activated).astype(jnp.bfloat16)
    input_part = lax.dot_general(
        gate_pre, w_gate, contract_last, preferred_element_type=jnp.float32
    )
    input_part = input_part + lax.dot_general(
        up_pre, w_up, contract_last, preferred_element_type=jnp.float32
    )
    input_part = input_part.astype(jnp.bfloat16).reshape(n_ep, capacity, model_width)
    share = lax.psum_scatter(input_part, "tp", scatter_dimension=2, tiled=True)

    down_sum = lax.dot_general(
        hidden, flat_scaled, contract_rows, preferred_element_type=jnp.float32
    )
    gate_sum = lax.dot_general(flat_in, gate_pre, contract_rows, preferred_element_type=jnp.float32)
    up_sum = lax.dot_general(flat_in, up_pre, contract_rows, preferred_element_type=jnp.float32)
    norm_part = (
        jnp.stack([jnp.sum(gate_sum * gate_sum, axis=1), jnp.sum(up_sum * up_sum, axis=1)])
        / hidden_total
    )
    down_norms = jnp.sum(down_sum * down_sum, axis=1) / model_width
    scores, row_norms = small_sums(score_part, norm_part, n_ep, n_tp)

    share, scores, row_norms, down_norms = lax.optimization_barrier(
        (share, scores, row_norms, down_norms)
    )
    returned = lax.all_to_all(share, "ep", split_axis=0, concat_axis=0, tiled=True)
    returned = returned.reshape(buffer_rows, -1)
    token_share = lax.dot_general(pick, returned, contract_rows, preferred_element_type=jnp.float32)
    token_grad = lax.all_gather(token_share.astype(jnp.bfloat16), "tp", axis=1, tiled=True)

    score_of = jnp.sum(jnp.where(filled, scores[:, :, None], 0.0), axis=1)
    slot_score = jnp.stack(
        [jnp.sum(jnp.where(p, score_of, 0.0), axis=0) for p in picks], axis=1
    ) / weight
    expert_prob_grad = group_prob[:, None] * slot_score
    group_prob_grad = jnp.sum(expert_prob * slot_score, axis=1)
    return (
        token_grad,
        group_prob_grad,
        expert_prob_grad,
        gate_sum.astype(jnp.bfloat16)[None],
        up_sum.astype(jnp.bfloat16)[None],
        down_sum.astype(jnp.bfloat16)[None],
        row_norms[0][None],
        row_norms[1][None],
        down_norms[None],
    )


def solution(mesh):
    return jax.shard_map(
        local,
        mesh=mesh,
        in_specs=(
            P("ep", None),
            P("ep", None),
            P("ep"),
            P("ep", None),
            P("ep", None),
            P("ep", None, "tp"),
            P("ep", None, "tp"),
            P("ep", "tp", None),
        ),
        out_specs=(
            P("ep", None),
            P("ep"),
            P("ep", None),
            P("ep", None, "tp"),
            P("ep", None, "tp"),
            P("ep", "tp", None),
            P("ep", None),
            P("ep", None),
            P("ep", "tp"),
        ),
        check_vma=False,
    )
```

time: 291 us -> 163 us (0.56)
  waiting for transfers between devices: 119 us -> 23.8 us
  Pallas kernels: 0 us -> 60.3 us
  blocking collectives: 38 us -> 10.1 us
  local copies, waits for them, and re-layouts: 45.9 us -> 18.1 us
  other arithmetic: 20.9 us -> 3.85 us
  starting transfers between devices: 13.7 us -> 0.08 us
  matrix products: 38.7 us -> 31.6 us
    pallas_call x0 -> x2, Pallas kernels: none -> 60.3 us  [the longest x1 43.1 us: dispatch(): pl.pallas_call(functools.partial(dispatch_kernel, n_ep), out_shape=jax.Sh...]
    reduce_scatter x1, waiting for transfers between devices: 70.1 us -> 11.5 us  [local(): share = lax.psum_scatter(input_part, 'tp', scatter_dimension=2, tiled=True)]
    all_to_all x3 -> x0, waiting for transfers between devices: 48.8 us -> none  [the longest x1 25.7 us: local(): lax.all_to_all(send_scaled, 'ep', split_axis=0, concat_axis=0, tiled=True)]
    gather x6 -> x0, local copies, waits for them, and re-layouts: 31.9 us -> none  [the longest x2 11.9 us: local(): per_slot = returned_rows.reshape(buffer_rows, model_width)[target]]
    psum x1 -> x0, blocking collectives: 28 us -> none  [local(): scores, row_norms = lax.psum((score_part, norm_part), 'tp')]
    all_to_all x3 -> x0, starting transfers between devices: 13.4 us -> none  [the longest x1 5.32 us: local(): lax.all_to_all(send_in, 'ep', split_axis=0, concat_axis=0, tiled=True)]
    all_gather x1, waiting for transfers between devices: 0.01 us -> 12.3 us  [local(): lax.all_gather(token_share.astype(jnp.bfloat16), 'tp', axis=1, tiled=True)]
    reduce_sum x2 -> x4, other arithmetic: 7.68 us -> 1.01 us  [the longest x1 0.58 us: local(): group_prob_grad = jnp.sum(expert_prob * slot_score, axis=1)]
  transfers between devices with their start and end apart: 5 -> 2, of which waited for: 3 -> 2; matrix products, arithmetic and copies ran while one was open for 18% -> 16% of each run, Pallas kernels for 0% -> 11%
where the time goes in v1:
time: 163 us; the launch traced here: 162 us
  Pallas kernels  60.3 us (37%)
  matrix products  31.6 us (19%)
  waiting for transfers between devices  23.8 us (15%)
  local copies, waits for them, and re-layouts  18.1 us (11%)
  between operations  14.2 us (9%)
  blocking collectives  10.1 us (6%)
  other arithmetic  3.85 us (2%)
    pallas_call x1, Pallas kernels, dispatch(): pl.pallas_call(functools.partial(dispatch_kernel, n_ep), out_shape=jax.Sh...  43.1 us
    pallas_call x1, Pallas kernels, small_sums(): pl.pallas_call(functools.partial(sums_kernel, n_ep, n_tp), out_shape=(jax...  17.2 us
    all_gather x1, waiting for transfers between devices, local(): lax.all_gather(token_share.astype(jnp.bfloat16), 'tp', axis=1, tiled=True)  12.3 us
    unnamed x22, local copies, waits for them, and re-layouts  12.3 us
    reduce_scatter x1, waiting for transfers between devices, local(): share = lax.psum_scatter(input_part, 'tp', scatter_dimension=2, tiled=True)  11.5 us
    all_to_all x1, blocking collectives, local(): lax.all_to_all(share, 'ep', split_axis=0, concat_axis=0, tiled=True)  10.1 us
    dot_general x1, matrix products, local(): lax.dot_general(flat_in, gate_pre, contract_rows, preferred_element_type=...  5.39 us
    dot_general x1, matrix products, local(): lax.dot_general(hidden, flat_scaled, contract_rows, preferred_element_typ...  5.32 us
  transfers between devices with their start and end apart: 2, of which 2 were waited for; matrix products, arithmetic and copies ran while one was open for 16% of the time, Pallas kernels for 11%

profile of v1, /device:TPU:0, one launch (start us, length us, event | category | flops | bytes accessed | tf_op | source)
XLA Modules:
  0.0 162.1 jit_solution(11941260770508540202)
XLA Ops:
  7.2 0.0 copy-start
  7.2 0.0 reduce-scatter.2.cloned.1.call-start
  7.2 0.8 broadcast_multiply_fusion.2
  8.1 0.8 fusion.22
  8.8 0.2 fusion.11
  9.0 0.2 select_reduce_fusion.1
  9.2 0.1 select_n.66
  9.3 0.1 iota.39
  9.4 0.2 bitcast_compare_fusion
  9.6 3.9 %multiply_convert_fusion = bf16[768,2048]{1,0:T(8,128)(2,1)} fusion(pred[768,256]{1,0:T(32,128)(4,1)S(1)} %bitcast_compare_fusion, f32[768]{0:T(1024)S(1)} %select_n.66, bf16[256,2048]{1,0:T(8,128)(2,1)} %param.8, bf16[256,2048]{1,0:T(8,128)(2,1)} %param.9, pred[]{:T(512)S(6)} %eq.67), kind=kOutput, calls=%fused_computation.1 | convolution fusion | flops 808976384 | bytes 5442561 | tf_op jit(solution)/shard_map/dot_general | solution.py:241
  13.5 43.1 %dispatch.1 = bf16[2,4,192,2048]{3,2,1,0:T(8,128)(2,1)} custom-call(bf16[4,192,2048]{2,1,0:T(8,128)(2,1)} %bitcast.64), custom_call_target="tpu_custom_call" | custom-call | tf_op jit(solution)/shard_map/dispatch/pallas_call | solution.py:87
  56.7 3.4 %fusion.19 = (bf16[1,4,192,2048]{3,2,1,0:T(8,128)(2,1)S(1)}, bf16[1,4,192,2048]{3,2,1,0:T(8,128)(2,1)S(1)}) fusion(bf16[2,4,192,2048]{3,2,1,0:T(8,128)(2,1)} %dispatch.1), kind=kLoop, calls=%fused_computation.52 | loop fusion | bytes 12582912 | tf_op jit(solution)/shard_map/slice | solution.py:245
  60.1 0.0 copy-start.2
  60.1 0.0 copy-start.1
  60.1 0.0 copy-done
  60.1 0.0 copy-start.4
  60.2 1.8 %fusion.2 = f32[768,512]{0,1:T(8,128)S(1)} fusion(bf16[768,2048]{1,0:T(8,128)(2,1)S(1)} %bitcast.60, bf16[1,2048,512]{2,1,0:T(8,128)(2,1)S(1)} %copy-done), kind=kOutput, calls=%fused_computation.7 | convolution fusion | flops 1610612736 | bytes 6815744 | tf_op jit(solution)/shard_map/dot_general | solution.py:253
  62.0 0.0 copy-done.2
  62.0 1.3 copy-done.4
  63.3 1.8 %fusion.5 = f32[768,512]{0,1:T(8,128)S(1)} fusion(bf16[768,2048]{1,0:T(8,128)(2,1)S(1)} %bitcast.61, bf16[1,2048,512]{2,1,0:T(8,128)(2,1)S(1)} %copy-done.4), kind=kOutput, calls=%fused_computation.10 | convolution fusion | flops 1610612736 | bytes 6815744 | tf_op jit(solution)/shard_map/dot_general | solution.py:254
  65.2 0.0 copy-done.1
  65.2 0.0 copy-done.8
  65.2 3.3 %multiply_reduce_fusion.3 = (f32[768]{0:T(1024)S(1)}, bf16[768,512]{0,1:T(8,128)(2,1)}, bf16[768,512]{0,1:T(8,128)(2,1)S(1)}, bf16[768,512]{0,1:T(8,128)(2,1)S(1)}) fusion(f32[768,512]{0,1:T(8,128)S(1)} %fusion.5, f32[768,512]{0,1:T(8,128)S(1)} %fusion.2, bf16[768,2048]{1,0:T(8,128)(2,1)S(1)} %bitcast.58, bf16[1,512,2048]{2,1,0:T(8,128)(2,1)S(1)} %copy-done.8), kind=kOutput, calls=%fused_computation.17 | convolution fusion | flops 1617689856 | bytes 10750976 | tf_op jit(solution)/shard_map/dot_general | solution.py:259
  68.5 1.8 %fusion = f32[768,2048]{1,0:T(8,128)S(1)} fusion(bf16[768,512]{0,1:T(8,128)(2,1)S(1)} %get-tuple-element.38, bf16[1,2048,512]{2,1,0:T(8,128)(2,1)S(1)} %copy-done), kind=kOutput, calls=%fused_computation.5 | convolution fusion | flops 1610612736 | bytes 9175040 | tf_op jit(solution)/shard_map/dot_general | solution.py:265
  70.3 3.8 %add_convert_fusion = bf16[768,2048]{1,0:T(8,128)(2,1)} fusion(f32[768,2048]{1,0:T(8,128)S(1)} %fusion, bf16[768,512]{0,1:T(8,128)(2,1)S(1)} %get-tuple-element.45, bf16[1,2048,512]{2,1,0:T(8,128)(2,1)S(1)} %copy-done.4), kind=kOutput, calls=%fused_computation | convolution fusion | flops 1613758464 | bytes 12320768 | tf_op jit(solution)/shard_map/dot_general | solution.py:268
  74.1 0.0 reduce-scatter.2.cloned.1.call-update
  74.1 0.0 all-gather.2.cloned.1.call-start
  74.2 0.1 reshape.131
  74.3 5.4 %convert_bitcast_fusion.2 = (bf16[1,2048,512]{1,2,0:T(8,128)(2,1)}, f32[2048]{0:T(1024)S(1)}) fusion(bf16[768,512]{0,1:T(8,128)(2,1)} %copy-done.5, bf16[768,2048]{1,0:T(8,128)(2,1)} %bitcast.62), kind=kOutput, calls=%fused_computation.16 | convolution fusion | flops 1613756416 | bytes 6037504 | tf_op jit(solution)/shard_map/dot_general | solution.py:277
  79.7 3.2 %convert_bitcast_fusion.1 = (bf16[1,2048,512]{1,2,0:T(8,128)(2,1)}, f32[2048]{0:T(1024)S(1)}) fusion(bf16[768,512]{0,1:T(8,128)(2,1)S(1)} %get-tuple-element.45, bf16[768,2048]{1,0:T(8,128)(2,1)S(1)} %bitcast.63), kind=kOutput, calls=%fused_computation.15 | convolution fusion | flops 1613756416 | bytes 6037504 | tf_op jit(solution)/shard_map/dot_general | solution.py:278
  82.9 0.6 pad_maximum_fusion.part_ref
  83.5 17.2 %small_sums.1 = (f32[32,128]{1,0:T(8,128)}, f32[4,8,128]{2,1,0:T(8,128)}) custom-call(f32[64,128]{1,0:T(8,128)} %pad_maximum_fusion.part_ref), custom_call_target="tpu_custom_call" | custom-call | bytes 20000000 | tf_op jit(solution)/shard_map/small_sums/pallas_call | solution.py:189
  100.7 0.7 copy.21
  101.4 0.7 reshape.134
  102.2 5.3 %convert_bitcast_fusion = (bf16[1,512,2048]{2,1,0:T(8,128)(2,1)}, f32[512]{0:T(512)S(1)}) fusion(bf16[768,512]{0,1:T(8,128)(2,1)} %get-tuple-element.35, bf16[768,2048]{1,0:T(8,128)(2,1)} %bitcast.59), kind=kOutput, calls=%fused_computation.14 | convolution fusion | flops 1613757952 | bytes 6031360 | tf_op jit(solution)/shard_map/dot_general | solution.py:274
  107.5 0.6 broadcast_multiply_fusion
  108.1 11.5 %reduce-scatter.2.cloned.1.call-done = bf16[4,192,256]{2,1,0:T(8,128)(2,1)} async-done(((bf16[4,192,2048]{2,1,0:T(8,128)(2,1)}), bf16[4,192,256]{2,1,0:T(8,128)(2,1)}) %reduce-scatter.2.cloned.1.call-update) | async-done | bytes 393232 | tf_op jit(solution)/shard_map/reduce_scatter | solution.py:272
  119.6 10.1 %all_to_all.5 = bf16[4,192,256]{2,1,0:T(8,128)(2,1)S(1)} all-to-all(bf16[4,192,256]{2,1,0:T(8,128)(2,1)} %reduce-scatter.2.cloned.1.call-done), channel_id=1, replica_groups=mesh['ep'=4,'tp'=8] {'ep'}, dimensions={0} | all-to-all | bytes 786432 | tf_op jit(solution)/shard_map/all_to_all | solution.py:289
  129.7 1.1 fusion.10
  130.8 0.0 all-gather.2.cloned.1.call-update
  130.8 3.9 %copy.18 = bf16[1,2048,512]{2,1,0:T(8,128)(2,1)} copy(bf16[1,2048,512]{1,2,0:T(8,128)(2,1)} %get-tuple-element.41) | data formatting | bytes 4194304
  134.7 4.0 %copy.17 = bf16[1,2048,512]{2,1,0:T(8,128)(2,1)} copy(bf16[1,2048,512]{1,2,0:T(8,128)(2,1)} %get-tuple-element.43) | data formatting | bytes 4194304
  138.7 0.2 select_reduce_fusion
  138.9 0.6 broadcast_multiply_fusion.1
  139.5 0.6 multiply_reduce_fusion.4
  140.1 0.6 fusion.20
  140.7 12.3 %all-gather.2.cloned.1.call-done = bf16[256,2048]{1,0:T(8,128)(2,1)} async-done(((bf16[256,256]{1,0:T(8,128)(2,1)}), bf16[256,2048]{1,0:T(8,128)(2,1)}) %all-gather.2.cloned.1.call-update) | async-done | bytes 1048592 | tf_op jit(solution)/shard_map/all_gather | solution.py:292
  153.0 2.3 %copy.25 = bf16[256,2048]{1,0:T(8,128)(2,1)} copy(bf16[256,2048]{1,0:T(8,128)(2,1)} %all-gather.2.cloned.1.call-done) | data formatting | bytes 2097152
  (19 shorter events, 0.1 us)
Async XLA Ops:
  7.2 53.0 %copy-start = (bf16[1,2048,512]{2,1,0:T(8,128)(2,1)S(1)}, bf16[1,2048,512]{2,1,0:T(8,128)(2,1)}, u32[]{:S(2)}) copy-start(bf16[1,2048,512]{2,1,0:T(8,128)(2,1)} %param.13) | copy-start | bytes 6291460
  7.2 112.4 %reduce-scatter.2.cloned.1.call-start = ((), (), s32[]{:S(2)}) async-start(), calls=%async_computation.2 | async-start | bytes 3538944 | tf_op jit(solution)/shard_map/reduce_scatter | solution.py:272
  60.1 1.9 %copy-start.2 = (bf16[1,4,192,2048]{3,2,1,0:T(8,128)(2,1)}, bf16[1,4,192,2048]{3,2,1,0:T(8,128)(2,1)S(1)}, u32[]{:S(2)}) copy-start(bf16[1,4,192,2048]{3,2,1,0:T(8,128)(2,1)S(1)} %get-tuple-element.37) | copy-start | bytes 9437188
  60.1 5.0 %copy-start.1 = (bf16[1,4,192,2048]{3,2,1,0:T(8,128)(2,1)}, bf16[1,4,192,2048]{3,2,1,0:T(8,128)(2,1)S(1)}, u32[]{:S(2)}) copy-start(bf16[1,4,192,2048]{3,2,1,0:T(8,128)(2,1)S(1)} %get-tuple-element.36) | copy-start | bytes 9437188
  60.1 3.2 %copy-start.4 = (bf16[1,2048,512]{2,1,0:T(8,128)(2,1)S(1)}, bf16[1,2048,512]{2,1,0:T(8,128)(2,1)}, u32[]{:S(2)}) copy-start(bf16[1,2048,512]{2,1,0:T(8,128)(2,1)} %param.14) | copy-start | bytes 6291460
  63.3 1.9 %copy-start.8 = (bf16[1,512,2048]{2,1,0:T(8,128)(2,1)S(1)}, bf16[1,512,2048]{2,1,0:T(8,128)(2,1)}, u32[]{:S(2)}) copy-start(bf16[1,512,2048]{2,1,0:T(8,128)(2,1)} %param.15) | copy-start | bytes 6291460
  68.5 1.9 %copy-start.5 = (bf16[768,512]{0,1:T(8,128)(2,1)}, bf16[768,512]{0,1:T(8,128)(2,1)S(1)}, u32[]{:S(2)}) copy-start(bf16[768,512]{0,1:T(8,128)(2,1)S(1)} %get-tuple-element.38) | copy-start | bytes 2359300
  74.1 78.9 %all-gather.2.cloned.1.call-start = ((), (), s32[]{:S(2)}) async-start(), calls=%async_computation.3 | async-start | bytes 1179648 | tf_op jit(solution)/shard_map/all_gather | solution.py:292
  74.3 5.4 %copy-start.3 = (bf16[1,4,192,2048]{3,2,1,0:T(8,128)(2,1)S(1)}, bf16[1,4,192,2048]{3,2,1,0:T(8,128)(2,1)}, u32[]{:S(2)}) copy-start(bf16[1,4,192,2048]{3,2,1,0:T(8,128)(2,1)} %copy-done.2) | copy-start | bytes 9437188
  134.7 4.2 %copy-start.6 = (f32[256,2]{0,1:T(2,128)S(1)}, f32[256,2]{0,1:T(2,128)}, u32[]{:S(2)}) copy-start(f32[256,2]{0,1:T(2,128)} %param.11) | copy-start | bytes 6148
  134.7 4.2 %copy-start.7 = (f32[256]{0:T(256)S(1)}, f32[256]{0:T(256)}, u32[]{:S(2)}) copy-start(f32[256]{0:T(256)} %param.10) | copy-start | bytes 3076
Sparse Core Ops, SparseCore 0:
  74.2 45.3 reduce-scatter.1
  130.9 22.0 all-gather.1

commit v2 on v1

--- a/solution.py
+++ b/solution.py
@@ -212,6 +212,339 @@
     return score_out.reshape(n_ep, 1024)[:, :cap], norm_out.reshape(2, width)
 
 
+def finish_kernel(
+    n_ep, n_tp, both_ref, gate_ref, up_ref, hid_ref, part_ref, score_ref, pick_ref,
+    out_ref, gate_out, up_out, down_out, norm_ref, down_norm_ref, score_out,
+    rows_in, rows_scaled, gate_v, up_v, hid_v, gate_g, up_g, down_g, norm_part,
+    s_slots, s_total, n_slots, bufs, accs, returned,
+    load_sem, store_sem, rs_send, rs_recv, ep_send, ep_recv, ag_send, ag_recv,
+    sc_send, sc_recv, sx_send, sx_recv, nm_send, nm_recv,
+):
+    me = lax.axis_index("ep")
+    t = lax.axis_index("tp")
+    cap, width = part_ref.shape[1], part_ref.shape[2]
+    ff = gate_v.shape[1]
+    tok = out_ref.shape[0]
+    levels = len(bufs)
+    bits = [lax.rem(t // (1 << s), 2) for s in range(levels)]
+    peers = [t + (1 - 2 * bits[s]) * (1 << s) for s in range(levels)]
+
+    def remote(src, dst, send, recv, device):
+        return pltpu.make_async_remote_copy(
+            src_ref=src, dst_ref=dst, send_sem=send, recv_sem=recv,
+            device_id=device, device_id_type=MESH,
+        )
+
+    loads = []
+    for b in range(n_ep):
+        loads.append(pltpu.make_async_copy(
+            both_ref.at[0, b], rows_in.at[pl.ds(b * cap, cap)], load_sem.at[len(loads)]))
+        loads.append(pltpu.make_async_copy(
+            both_ref.at[1, b], rows_scaled.at[pl.ds(b * cap, cap)], load_sem.at[len(loads)]))
+    for src, dst in ((gate_ref, gate_v), (up_ref, up_v), (hid_ref, hid_v)):
+        loads.append(pltpu.make_async_copy(src, dst, load_sem.at[len(loads)]))
+
+    barrier = pltpu.get_barrier_semaphore()
+    for d in range(1, n_tp):
+        pl.semaphore_signal(
+            barrier, inc=1, device_id={"tp": lax.rem(t + d, n_tp)}, device_id_type=MESH
+        )
+    for d in range(1, n_ep):
+        pl.semaphore_signal(
+            barrier, inc=1, device_id={"ep": lax.rem(me + d, n_ep)}, device_id_type=MESH
+        )
+    pl.semaphore_wait(barrier, n_tp - 1 + n_ep - 1)
+
+    order = sorted(range(1, n_ep), key=lambda d: abs(d - n_ep // 2)) + [0]
+
+    def block(i):
+        return lax.rem(me + order[i], n_ep)
+
+    def halves(s):
+        w = width >> (s + 1)
+        keep = pl.ds(pl.multiple_of(bits[s] * w, 128), w)
+        give = pl.ds(pl.multiple_of((1 - bits[s]) * w, 128), w)
+        return keep, give
+
+    def exchange(s, i):
+        _, give = halves(s)
+        src = part_ref.at[block(i), :, give] if s == 0 else accs[s - 1].at[i, :, give]
+        return remote(src, bufs[s].at[i], rs_send.at[s, i], rs_recv.at[s, i], {"tp": peers[s]})
+
+    def to_owner(i):
+        d = order[i]
+        return remote(
+            accs[levels - 1].at[i],
+            returned.at[pl.ds(pl.multiple_of(me * cap, 16), cap)],
+            ep_send.at[d], ep_recv.at[d], {"ep": block(i)},
+        )
+
+    def from_owner(d):
+        src = lax.rem(me - d + n_ep, n_ep)
+        return remote(
+            accs[levels - 1].at[0],
+            returned.at[pl.ds(pl.multiple_of(src * cap, 16), cap)],
+            ep_send.at[d], ep_recv.at[d], {"ep": src},
+        )
+
+    def score_to(d):
+        return remote(score_ref, s_slots.at[t], sc_send.at[d], sc_recv.at[d],
+                      {"tp": lax.rem(t + d, n_tp)})
+
+    def score_from(d):
+        src = lax.rem(t - d + n_tp, n_tp)
+        return remote(score_ref, s_slots.at[src], sc_send.at[d], sc_recv.at[d], {"tp": src})
+
+    def norm_to(d):
+        return remote(norm_part, n_slots.at[t], nm_send.at[d], nm_recv.at[d],
+                      {"tp": lax.rem(t + d, n_tp)})
+
+    def norm_from(d):
+        src = lax.rem(t - d + n_tp, n_tp)
+        return remote(norm_part, n_slots.at[src], nm_send.at[d], nm_recv.at[d], {"tp": src})
+
+    def score_back(d):
+        dst = lax.rem(me + d, n_ep)
+        return remote(s_total.at[pl.ds(pl.multiple_of(dst * 8, 8), 8)], score_out.at[me],
+                      sx_send.at[d], sx_recv.at[d], {"ep": dst})
+
+    def score_arrive(d):
+        src = lax.rem(me - d + n_ep, n_ep)
+        return remote(s_total.at[pl.ds(0, 8)], score_out.at[src],
+                      sx_send.at[d], sx_recv.at[d], {"ep": src})
+
+    for i in range(n_ep):
+        exchange(0, i).start()
+    for d in range(1, n_tp):
+        score_to(d).start()
+    for copy in loads:
+        copy.start()
+    s_slots[t] = score_ref[...]
+
+    rows = (((0,), (0,)), ((), ()))
+    step = 256
+    half = width // step // 2
+
+    def fold(sq):
+        parts = [sq[:, j * 128:(j + 1) * 128] for j in range(sq.shape[1] // 128)]
+        return functools.reduce(jnp.add, parts)
+
+    def line(x):
+        return jnp.sum(jnp.transpose(x), axis=0, keepdims=True)
+
+    def gate_up(first):
+        def body(j, carry):
+            at = pl.ds(pl.multiple_of(j * step, step), step)
+            lhs = rows_in[:, at]
+            for n, (rhs, out) in enumerate(((gate_v, gate_g), (up_v, up_g))):
+                total = lax.dot_general(lhs, rhs[...], rows, preferred_element_type=jnp.float32)
+                out[at, :] = total.astype(jnp.bfloat16)
+                sq = fold(total * total)
+                for h in range(step // 128):
+                    norm_part[n, pl.ds(j * (step // 128) + h, 1), :] = line(
+                        sq[h * 128:(h + 1) * 128]
+                    ) / (ff * n_tp)
+            return carry
+        lax.fori_loop(first, first + half, body, 0)
+
+    def down():
+        def body(j, carry):
+            at = pl.ds(pl.multiple_of(j * step, step), step)
+            lhs = hid_v[:, at]
+            sq = None
+            for c in range(0, width, 512):
+                total = lax.dot_general(
+                    lhs, rows_scaled[:, c:c + 512], rows, preferred_element_type=jnp.float32
+                )
+                down_g[at, c:c + 512] = total.astype(jnp.bfloat16)
+                more = fold(total * total)
+                sq = more if sq is None else sq + more
+            for h in range(step // 128):
+                down_norm_ref[pl.ds(j * (step // 128) + h, 1), :] = line(
+                    sq[h * 128:(h + 1) * 128]
+                ) / width
+            return carry
+        lax.fori_loop(0, ff // step, body, 0)
+
+    stores = [
+        pltpu.make_async_copy(a, b, store_sem.at[n])
+        for n, (a, b) in enumerate(((gate_g, gate_out), (up_g, up_out), (down_g, down_out)))
+    ]
+
+    def work_first():
+        for copy in loads:
+            copy.wait()
+        gate_up(0)
+
+    def work_second():
+        gate_up(half)
+        for d in range(1, n_tp):
+            norm_to(d).start()
+        n_slots[t] = norm_part[...]
+        stores[0].start()
+        stores[1].start()
+
+    def work_third():
+        for d in range(1, n_tp):
+            score_from(d).wait_recv()
+        acc = s_slots[0]
+        for i in range(1, n_tp):
+            acc = acc + s_slots[i]
+        s_total[...] = acc
+        down()
+        stores[2].start()
+        for d in range(1, n_ep):
+            score_back(d).start()
+        score_out[me] = s_total[pl.ds(pl.multiple_of(me * 8, 8), 8)]
+
+    work = [work_first, work_second, work_third]
+    for tick in range(max(n_ep + levels - 1, len(work))):
+        for i in range(n_ep):
+            s = tick - i
+            if not 0 <= s < levels:
+                continue
+            exchange(s, i).wait_recv()
+            keep, _ = halves(s)
+            own = part_ref[block(i), :, keep] if s == 0 else accs[s - 1][i, :, keep]
+            total = own.astype(jnp.float32) + bufs[s][i].astype(jnp.float32)
+            accs[s][i] = total.astype(jnp.bfloat16)
+            if s + 1 < levels:
+                exchange(s + 1, i).start()
+            elif order[i]:
+                to_owner(i).start()
+            else:
+                returned[pl.ds(pl.multiple_of(me * cap, 16), cap), :] = total.astype(jnp.bfloat16)
+        if tick < len(work):
+            work[tick]()
+
+    for d in range(1, n_ep):
+        from_owner(d).wait_recv()
+    share = width >> levels
+    base = [None] * (levels + 1)
+    base[0] = 0
+    for s in range(levels):
+        base[s + 1] = base[s] + bits[s] * (width >> (s + 1))
+    pieces = 2
+    piece = tok // pieces
+
+    def spread(s, p):
+        w = width >> (s + 1)
+        at = pl.ds(pl.multiple_of(base[s + 1], 128), w)
+        ref = out_ref.at[pl.ds(p * piece, piece), at]
+        return remote(ref, ref, ag_send.at[s, p], ag_recv.at[s, p], {"tp": peers[s]})
+
+    def arrived(s, p):
+        w = width >> (s + 1)
+        at = pl.ds(pl.multiple_of(base[s] + (1 - bits[s]) * w, 128), w)
+        ref = out_ref.at[pl.ds(p * piece, piece), at]
+        return remote(ref, ref, ag_send.at[s, p], ag_recv.at[s, p], {"tp": peers[s]})
+
+    for p in range(pieces):
+        grad = jnp.dot(
+            pick_ref[p * piece:(p + 1) * piece, :], returned[...],
+            preferred_element_type=jnp.float32,
+        )
+        out_ref[p * piece:(p + 1) * piece, pl.ds(pl.multiple_of(base[levels], 128), share)] = (
+            grad.astype(jnp.bfloat16)
+        )
+        spread(levels - 1, p).start()
+    for d in range(1, n_tp):
+        norm_from(d).wait_recv()
+    acc = n_slots[0]
+    for i in range(1, n_tp):
+        acc = acc + n_slots[i]
+    norm_ref[...] = acc
+    for s in reversed(range(levels)):
+        for p in range(pieces):
+            arrived(s, p).wait_recv()
+            if s:
+                spread(s - 1, p).start()
+
+    for d in range(1, n_ep):
+        score_arrive(d).wait_recv()
+        score_back(d).wait_send()
+    for i in range(n_ep):
+        for s in range(levels):
+            exchange(s, i).wait_send()
+        if order[i]:
+            to_owner(i).wait_send()
+    for d in range(1, n_tp):
+        score_to(d).wait_send()
+        norm_to(d).wait_send()
+    for s in range(levels):
+        for p in range(pieces):
+            spread(s, p).wait_send()
+    for copy in stores:
+        copy.wait()
+
+
+def finish(both, gate_pre, up_pre, hidden, part, score_part, pick_t, n_ep, n_tp):
+    cap, width = part.shape[1:]
+    rows, ff = gate_pre.shape
+    tok = pick_t.shape[0]
+    levels = n_tp.bit_length() - 1
+    scores = jnp.pad(score_part, ((0, 0), (0, 1024 - cap))).reshape(n_ep * 8, 128)
+    bf, f32 = jnp.bfloat16, jnp.float32
+    vmem = pl.BlockSpec(memory_space=pltpu.VMEM)
+    hbm = pl.BlockSpec(memory_space=pl.ANY)
+    dma = pltpu.SemaphoreType.DMA
+    stages = [pltpu.VMEM((n_ep, cap, width >> (s + 1)), bf) for s in range(levels)]
+    outs = pl.pallas_call(
+        functools.partial(finish_kernel, n_ep, n_tp),
+        out_shape=(
+            jax.ShapeDtypeStruct((tok, width), bf),
+            jax.ShapeDtypeStruct((width, ff), bf),
+            jax.ShapeDtypeStruct((width, ff), bf),
+            jax.ShapeDtypeStruct((ff, width), bf),
+            jax.ShapeDtypeStruct((2, width // 128, 128), f32),
+            jax.ShapeDtypeStruct((ff // 128, 128), f32),
+            jax.ShapeDtypeStruct((n_ep, 8, 128), f32),
+        ),
+        in_specs=[hbm, hbm, hbm, hbm, vmem, vmem, vmem],
+        out_specs=(vmem, hbm, hbm, hbm, vmem, vmem, vmem),
+        scratch_shapes=[
+            pltpu.VMEM((rows, width), bf),
+            pltpu.VMEM((rows, width), bf),
+            pltpu.VMEM((rows, ff), bf),
+            pltpu.VMEM((rows, ff), bf),
+            pltpu.VMEM((rows, ff), bf),
+            pltpu.VMEM((width, ff), bf),
+            pltpu.VMEM((width, ff), bf),
+            pltpu.VMEM((ff, width), bf),
+            pltpu.VMEM((2, width // 128, 128), f32),
+            pltpu.VMEM((n_tp,) + scores.shape, f32),
+            pltpu.VMEM(scores.shape, f32),
+            pltpu.VMEM((n_tp, 2, width // 128, 128), f32),
+            list(stages),
+            list(stages),
+            pltpu.VMEM((rows, width >> levels), bf),
+            dma((2 * n_ep + 3,)),
+            dma((3,)),
+            dma((levels, n_ep)),
+            dma((levels, n_ep)),
+            dma((n_ep,)),
+            dma((n_ep,)),
+            dma((levels, 2)),
+            dma((levels, 2)),
+            dma((n_tp,)),
+            dma((n_tp,)),
+            dma((n_ep,)),
+            dma((n_ep,)),
+            dma((n_tp,)),
+            dma((n_tp,)),
+        ],
+        compiler_params=pltpu.CompilerParams(
+            collective_id=2, has_side_effects=True, vmem_limit_bytes=48 << 20
+        ),
+        name="finish",
+    )(both, gate_pre, up_pre, hidden, part, scores, pick_t)
+    token_grad, gate_g, up_g, down_g, norms, down_norms, score_out = outs
+    return (
+        token_grad, gate_g, up_g, down_g, norms.reshape(2, width),
+        down_norms.reshape(ff), score_out.reshape(n_ep, 1024)[:, :cap],
+    )
+
+
 def local(tokens, cotangent, group_prob, expert_prob, routing, gate_weight, up_weight, down_weight):
     tok_count, model_width = tokens.shape
     top_count = routing.shape[1]
@@ -269,27 +602,36 @@
         up_pre, w_up, contract_last, preferred_element_type=jnp.float32
     )
     input_part = input_part.astype(jnp.bfloat16).reshape(n_ep, capacity, model_width)
-    share = lax.psum_scatter(input_part, "tp", scatter_dimension=2, tiled=True)
-
-    down_sum = lax.dot_general(
-        hidden, flat_scaled, contract_rows, preferred_element_type=jnp.float32
-    )
-    gate_sum = lax.dot_general(flat_in, gate_pre, contract_rows, preferred_element_type=jnp.float32)
-    up_sum = lax.dot_general(flat_in, up_pre, contract_rows, preferred_element_type=jnp.float32)
-    norm_part = (
-        jnp.stack([jnp.sum(gate_sum * gate_sum, axis=1), jnp.sum(up_sum * up_sum, axis=1)])
-        / hidden_total
-    )
-    down_norms = jnp.sum(down_sum * down_sum, axis=1) / model_width
-    scores, row_norms = small_sums(score_part, norm_part, n_ep, n_tp)
-
-    share, scores, row_norms, down_norms = lax.optimization_barrier(
-        (share, scores, row_norms, down_norms)
-    )
-    returned = lax.all_to_all(share, "ep", split_axis=0, concat_axis=0, tiled=True)
-    returned = returned.reshape(buffer_rows, -1)
-    token_share = lax.dot_general(pick, returned, contract_rows, preferred_element_type=jnp.float32)
-    token_grad = lax.all_gather(token_share.astype(jnp.bfloat16), "tp", axis=1, tiled=True)
+    if n_tp & (n_tp - 1) == 0 and model_width // n_tp % 128 == 0:
+        pick_t = pick.T
+        token_grad, gate_grad, up_grad, down_grad, row_norms, down_norms, scores = finish(
+            both, gate_pre, up_pre, hidden, input_part, score_part, pick_t, n_ep, n_tp
+        )
+    else:
+        share = lax.psum_scatter(input_part, "tp", scatter_dimension=2, tiled=True)
+
+        down_sum = lax.dot_general(
+            hidden, flat_scaled, contract_rows, preferred_element_type=jnp.float32
+        )
+        gate_sum = lax.dot_general(flat_in, gate_pre, contract_rows, preferred_element_type=jnp.float32)
+        up_sum = lax.dot_general(flat_in, up_pre, contract_rows, preferred_element_type=jnp.float32)
+        norm_part = (
+            jnp.stack([jnp.sum(gate_sum * gate_sum, axis=1), jnp.sum(up_sum * up_sum, axis=1)])
+            / hidden_total
+        )
+        down_norms = jnp.sum(down_sum * down_sum, axis=1) / model_width
+        scores, row_norms = small_sums(score_part, norm_part, n_ep, n_tp)
+
+        share, scores, row_norms, down_norms = lax.optimization_barrier(
+            (share, scores, row_norms, down_norms)
+        )
+        returned = lax.all_to_all(share, "ep", split_axis=0, concat_axis=0, tiled=True)
+        returned = returned.reshape(buffer_rows, -1)
+        token_share = lax.dot_general(pick, returned, contract_rows, preferred_element_type=jnp.float32)
+        token_grad = lax.all_gather(token_share.astype(jnp.bfloat16), "tp", axis=1, tiled=True)
+        gate_grad, up_grad, down_grad = (
+            x.astype(jnp.bfloat16) for x in (gate_sum, up_sum, down_sum)
+        )
 
     score_of = jnp.sum(jnp.where(filled, scores[:, :, None], 0.0), axis=1)
     slot_score = jnp.stack(
@@ -301,9 +643,9 @@
         token_grad,
         group_prob_grad,
         expert_prob_grad,
-        gate_sum.astype(jnp.bfloat16)[None],
-        up_sum.astype(jnp.bfloat16)[None],
-        down_sum.astype(jnp.bfloat16)[None],
+        gate_grad[None],
+        up_grad[None],
+        down_grad[None],
         row_norms[0][None],
         row_norms[1][None],
         down_norms[None],

time: 163 us -> 135 us (0.83)
  Pallas kernels: 60.3 us -> 99.3 us
  waiting for transfers between devices: 23.8 us -> 0 us
  matrix products: 31.6 us -> 16.6 us
  between operations: 14.2 us -> 0.83 us
  blocking collectives: 10.1 us -> 0 us
  local copies, waits for them, and re-layouts: 18.1 us -> 13.9 us
    pallas_call x1, Pallas kernels: 17.2 us -> 56.1 us  [finish(): pl.pallas_call(functools.partial(finish_kernel, n_ep, n_tp), out_shape=(j...]
    dot_general x4 -> x0, matrix products: 15 us -> none  [the longest x1 5.39 us: local(): lax.dot_general(flat_in, gate_pre, contract_rows, preferred_element_type=...]
    all_gather x1 -> x0, waiting for transfers between devices: 12.3 us -> none  [local(): lax.all_gather(token_share.astype(jnp.bfloat16), 'tp', axis=1, tiled=True)]
    reduce_scatter x1 -> x0, waiting for transfers between devices: 11.5 us -> none  [local(): share = lax.psum_scatter(input_part, 'tp', scatter_dimension=2, tiled=True)]
    all_to_all x1 -> x0, blocking collectives: 10.1 us -> none  [local(): lax.all_to_all(share, 'ep', split_axis=0, concat_axis=0, tiled=True)]
    unnamed x22 -> x26, local copies, waits for them, and re-layouts: 12.3 us -> 7.61 us
  transfers between devices with their start and end apart: 2 -> 0, of which waited for: 2 -> 0; matrix products, arithmetic and copies ran while one was open for 16% -> 0% of each run, Pallas kernels for 11% -> 0%
where the time goes in v2:
time: 135 us; the launch traced here: 134 us
  Pallas kernels  99.3 us (74%)
  matrix products  16.6 us (12%)
  local copies, waits for them, and re-layouts  13.9 us (10%)
  other arithmetic  3.74 us (3%)
    pallas_call x1, Pallas kernels, finish(): pl.pallas_call(functools.partial(finish_kernel, n_ep, n_tp), out_shape=(j...  56.1 us
    pallas_call x1, Pallas kernels, dispatch(): pl.pallas_call(functools.partial(dispatch_kernel, n_ep), out_shape=jax.Sh...  43.1 us
    unnamed x26, local copies, waits for them, and re-layouts  7.61 us
    dot_general x1, matrix products, local(): mine = jnp.dot(pick, source, preferred_element_type=jnp.float32) * factor  3.99 us
    dot_general x1, matrix products, local(): lax.dot_general(flat_scaled, w_down, contract_last, preferred_element_typ...  3.57 us
    dot_general x1, matrix products, local(): lax.dot_general(up_pre, w_up, contract_last, preferred_element_type=jnp.f...  3.52 us
    slice x1, local copies, waits for them, and re-layouts, local(): flat_scaled = both[1].reshape(buffer_rows, model_width)  3.43 us

profile of v2, /device:TPU:0, one launch (start us, length us, event | category | flops | bytes accessed | tf_op | source)
XLA Modules:
  0.0 134.3 jit_solution(9454380974650764295)
XLA Ops:
  0.6 0.0 copy-start
  0.7 0.8 broadcast_multiply_fusion.1
  1.5 0.8 fusion.20
  2.3 0.2 fusion.10
  2.4 0.2 select_reduce_fusion.1
  2.7 0.1 select_n.66
  2.8 0.1 iota.40
  2.8 0.1 eq.64
  2.9 1.1 copy.27
  4.1 1.3 convert_bitcast_fusion
  5.3 4.0 %multiply_convert_fusion = bf16[768,2048]{1,0:T(8,128)(2,1)} fusion(pred[768,256]{0,1:T(32,128)(4,1)S(1)} %get-tuple-element.28, f32[768]{0:T(1024)S(1)} %select_n.66, bf16[256,2048]{1,0:T(8,128)(2,1)} %param.8, bf16[256,2048]{1,0:T(8,128)(2,1)} %param.9, pred[]{:T(512)S(6)} %eq.67), kind=kOutput, calls=%fused_computation.1 | convolution fusion | flops 808976384 | bytes 5442561 | tf_op jit(solution)/shard_map/dot_general | solution.py:574
  9.3 43.1 %dispatch.1.both_ref = bf16[2,4,192,2048]{3,2,1,0:T(8,128)(2,1)} custom-call(bf16[4,192,2048]{2,1,0:T(8,128)(2,1)} %bitcast.50), custom_call_target="tpu_custom_call" | custom-call | tf_op jit(solution)/shard_map/dispatch/pallas_call | solution.py:87
  52.5 3.4 %fusion.17 = (bf16[1,4,192,2048]{3,2,1,0:T(8,128)(2,1)S(1)}, bf16[1,4,192,2048]{3,2,1,0:T(8,128)(2,1)S(1)}) fusion(bf16[2,4,192,2048]{3,2,1,0:T(8,128)(2,1)} %dispatch.1.both_ref), kind=kLoop, calls=%fused_computation.41 | loop fusion | bytes 12582912 | tf_op jit(solution)/shard_map/slice | solution.py:578
  55.9 0.0 copy-done
  55.9 0.0 copy-start.5
  55.9 1.8 %fusion.2 = f32[768,512]{1,0:T(8,128)S(1)} fusion(bf16[768,2048]{1,0:T(8,128)(2,1)S(1)} %bitcast.51, bf16[1,2048,512]{2,1,0:T(8,128)(2,1)S(1)} %copy-done), kind=kOutput, calls=%fused_computation.4 | convolution fusion | flops 1610612736 | bytes 6815744 | tf_op jit(solution)/shard_map/dot_general | solution.py:586
  57.7 0.0 copy-done.5
  57.7 0.0 copy-start.9
  57.7 1.8 %fusion.5 = f32[768,512]{1,0:T(8,128)S(1)} fusion(bf16[768,2048]{1,0:T(8,128)(2,1)S(1)} %bitcast.52, bf16[1,2048,512]{2,1,0:T(8,128)(2,1)S(1)} %copy-done.5), kind=kOutput, calls=%fused_computation.7 | convolution fusion | flops 1610612736 | bytes 6815744 | tf_op jit(solution)/shard_map/dot_general | solution.py:587
  59.5 0.0 copy-done.9
  59.5 3.6 %multiply_reduce_fusion = (f32[768]{0:T(1024)S(1)}, bf16[768,512]{1,0:T(8,128)(2,1)}, bf16[768,512]{1,0:T(8,128)(2,1)S(1)}, bf16[768,512]{1,0:T(8,128)(2,1)}) fusion(f32[768,512]{1,0:T(8,128)S(1)} %fusion.5, f32[768,512]{1,0:T(8,128)S(1)} %fusion.2, bf16[768,2048]{1,0:T(8,128)(2,1)S(1)} %bitcast.49, bf16[1,512,2048]{2,1,0:T(8,128)(2,1)S(1)} %copy-done.9), kind=kOutput, calls=%fused_computation.11 | convolution fusion | flops 1617689856 | bytes 10750976 | tf_op jit(solution)/shard_map/dot_general | solution.py:592
  63.1 0.1 reshape.128
  63.2 0.0 copy-start.1
  63.2 0.0 copy-start.6
  63.2 1.8 %fusion = f32[768,2048]{1,0:T(8,128)S(1)} fusion(bf16[768,512]{1,0:T(8,128)(2,1)S(1)} %get-tuple-element.33.gate_ref, bf16[1,2048,512]{2,1,0:T(8,128)(2,1)S(1)} %copy-done), kind=kOutput, calls=%fused_computation.2 | convolution fusion | flops 1610612736 | bytes 9175040 | tf_op jit(solution)/shard_map/dot_general | solution.py:598
  65.1 0.0 copy-done.1
  65.1 0.0 copy-done.6
  65.1 0.0 copy-start.2
  65.1 3.5 %add_convert_fusion = bf16[768,2048]{1,0:T(8,128)(2,1)} fusion(f32[768,2048]{1,0:T(8,128)S(1)} %fusion, bf16[768,512]{1,0:T(8,128)(2,1)S(1)} %copy-done.1, bf16[1,2048,512]{2,1,0:T(8,128)(2,1)S(1)} %copy-done.6), kind=kOutput, calls=%fused_computation | convolution fusion | flops 1613758464 | bytes 12320768 | tf_op jit(solution)/shard_map/dot_general | solution.py:601
  68.6 0.0 copy-done.2
  68.6 0.0 copy-start.7
  68.6 0.0 copy-start.8
  68.6 56.1 %finish.1 = (bf16[256,2048]{1,0:T(8,128)(2,1)S(1)}, bf16[2048,512]{1,0:T(8,128)(2,1)S(1)}, bf16[2048,512]{1,0:T(8,128)(2,1)}, bf16[512,2048]{1,0:T(8,128)(2,1)},...) custom-call(bf16[2,4,192,2048]{3,2,1,0:T(8,128)(2,1)} %dispatch.1.both_ref, ...), custom_call_target="tpu_custom_call" | custom-call | tf_op jit(solution)/shard_map/finish/pallas_call | solution.py:492
  124.8 0.2 select_reduce_fusion
  125.0 0.0 copy-done.7
  125.0 0.0 copy-done.8
  125.0 0.6 broadcast_multiply_fusion
  125.6 0.6 multiply_reduce_fusion.1
  126.2 0.6 fusion.18
  126.8 1.0 copy.49
  127.8 0.0 copy-start.4
  127.8 1.3 copy.50
  129.1 1.0 copy-done.4
  130.1 0.0 copy-start.3
  130.1 1.3 copy.51
  131.4 1.0 copy-done.3
  132.5 1.3 copy.52
  133.8 0.6 copy.53
  (9 shorter events, 0.1 us)
Async XLA Ops:
  0.6 55.3 %copy-start = (bf16[1,2048,512]{2,1,0:T(8,128)(2,1)S(1)}, bf16[1,2048,512]{2,1,0:T(8,128)(2,1)}, u32[]{:S(2)}) copy-start(bf16[1,2048,512]{2,1,0:T(8,128)(2,1)} %param.13) | copy-start | bytes 6291460
  55.9 1.8 %copy-start.5 = (bf16[1,2048,512]{2,1,0:T(8,128)(2,1)S(1)}, bf16[1,2048,512]{2,1,0:T(8,128)(2,1)}, u32[]{:S(2)}) copy-start(bf16[1,2048,512]{2,1,0:T(8,128)(2,1)} %param.14) | copy-start | bytes 6291460
  57.7 1.8 %copy-start.9 = (bf16[1,512,2048]{2,1,0:T(8,128)(2,1)S(1)}, bf16[1,512,2048]{2,1,0:T(8,128)(2,1)}, u32[]{:S(2)}) copy-start(bf16[1,512,2048]{2,1,0:T(8,128)(2,1)} %param.15) | copy-start | bytes 6291460
  63.2 1.9 %copy-start.1 = (bf16[768,512]{1,0:T(8,128)(2,1)S(1)}, bf16[768,512]{1,0:T(8,128)(2,1)}, u32[]{:S(2)}) copy-start(bf16[768,512]{1,0:T(8,128)(2,1)} %get-tuple-element.34.up_ref) | copy-start | bytes 2359300
  63.2 1.9 %copy-start.6 = (bf16[1,2048,512]{2,1,0:T(8,128)(2,1)S(1)}, bf16[1,2048,512]{2,1,0:T(8,128)(2,1)}, u32[]{:S(2)}) copy-start(bf16[1,2048,512]{2,1,0:T(8,128)(2,1)} %param.14) | copy-start | bytes 6291460
  65.1 3.5 %copy-start.2 = (bf16[768,512]{1,0:T(8,128)(2,1)S(1)}, bf16[768,512]{1,0:T(8,128)(2,1)}, u32[]{:S(2)}) copy-start(bf16[768,512]{1,0:T(8,128)(2,1)} %get-tuple-element.30.hid_ref) | copy-start | bytes 2359300
  68.6 56.4 %copy-start.7 = (f32[256,2]{0,1:T(2,128)S(1)}, f32[256,2]{0,1:T(2,128)}, u32[]{:S(2)}) copy-start(f32[256,2]{0,1:T(2,128)} %param.11) | copy-start | bytes 6148
  68.6 56.4 %copy-start.8 = (f32[256]{0:T(256)S(1)}, f32[256]{0:T(256)}, u32[]{:S(2)}) copy-start(f32[256]{0:T(256)} %param.10) | copy-start | bytes 3076
  127.8 2.3 %copy-start.4 = (bf16[2048,512]{1,0:T(8,128)(2,1)S(1)}, bf16[2048,512]{1,0:T(8,128)(2,1)}, u32[]{:S(2)}) copy-start(bf16[2048,512]{1,0:T(8,128)(2,1)} %get-tuple-element.19) | copy-start | bytes 6291460
  130.1 2.3 %copy-start.3 = (bf16[512,2048]{1,0:T(8,128)(2,1)S(1)}, bf16[512,2048]{1,0:T(8,128)(2,1)}, u32[]{:S(2)}) copy-start(bf16[512,2048]{1,0:T(8,128)(2,1)} %get-tuple-element.20) | copy-start | bytes 6291460

commit v3 on v2

--- a/solution.py
+++ b/solution.py
@@ -7,14 +7,17 @@
 from jax.sharding import PartitionSpec as P
 
 MESH = pl.DeviceIdType.MESH
-CHUNKS = 4
-
-
-def dispatch_kernel(n_ep, mine_ref, out_ref, local_sem, send_sem, recv_sem, fwd_send, fwd_recv):
+CHUNKS = 8
+DIRECT = 5
+
+
+def dispatch_kernel(n_ep, mine_ref, out_ref, local_sem, send_sem, recv_sem, fwd_send, fwd_recv, z_send, z_recv):
     me = lax.axis_index("ep")
     t = lax.axis_index("tp")
     core = lax.rem(t, 2)
     partner = t + 1 - 2 * core
+    side_z = lax.rem(t // 2, 2)
+    across = t + 2 - 4 * side_z
     width = mine_ref.shape[2] // CHUNKS
     barrier = pltpu.get_barrier_semaphore()
     for d in range(1, n_ep):
@@ -22,10 +25,13 @@
             barrier, inc=1, device_id={"ep": lax.rem(me + d, n_ep)}, device_id_type=MESH
         )
     pl.semaphore_signal(barrier, inc=1, device_id={"tp": partner}, device_id_type=MESH)
-    pl.semaphore_wait(barrier, n_ep)
+    pl.semaphore_signal(barrier, inc=1, device_id={"tp": across}, device_id_type=MESH)
+    pl.semaphore_wait(barrier, n_ep + 1)
 
     def cols(c):
-        return pl.ds(c * width, width)
+        j, side = (c, side_z) if c < DIRECT else (c - DIRECT, 1 - side_z)
+        at = j + side * (CHUNKS - 1 - 2 * j)
+        return pl.ds(pl.multiple_of(at * width, 128), width)
 
     def to_peer(d, c):
         dst = lax.rem(me + d, n_ep)
@@ -61,22 +67,45 @@
             device_id_type=MESH,
         )
 
+    def swap(d, c, arriving):
+        src = lax.rem(me - d + n_ep, n_ep)
+        ref = out_ref.at[core, src, :, cols(c + DIRECT if arriving else c)]
+        return pltpu.make_async_remote_copy(
+            src_ref=ref,
+            dst_ref=ref,
+            send_sem=z_send.at[d, c],
+            recv_sem=z_recv.at[d, c],
+            device_id={"tp": across},
+            device_id_type=MESH,
+        )
+
     order = sorted(range(1, n_ep), key=lambda d: abs(d - n_ep // 2))
-    for c in range(CHUNKS):
+    extra = CHUNKS - DIRECT
+    for c in range(DIRECT):
         for d in order:
             to_peer(d, c).start()
     keep = pltpu.make_async_copy(mine_ref.at[me], out_ref.at[core, me], local_sem)
     keep.start()
     for c in range(CHUNKS):
         forward(0, c, core).start()
-    for c in range(CHUNKS):
+    lag = DIRECT - extra
+    for c in range(DIRECT):
         for d in order:
             from_peer(d, c).wait_recv()
+            if c < extra:
+                swap(d, c, False).start()
             forward(d, c, core).start()
+        if c >= lag:
+            for d in order:
+                swap(d, c - lag, True).wait_recv()
+                forward(d, c - lag + DIRECT, core).start()
     keep.wait()
-    for c in range(CHUNKS):
+    for c in range(DIRECT):
         for d in order:
             to_peer(d, c).wait_send()
+    for c in range(extra):
+        for d in order:
+            swap(d, c, False).wait_send()
     for d in range(n_ep):
         for c in range(CHUNKS):
             forward(d, c, core).wait_send()
@@ -91,6 +120,8 @@
         out_specs=pl.BlockSpec(memory_space=pl.ANY),
         scratch_shapes=[
             pltpu.SemaphoreType.DMA,
+            pltpu.SemaphoreType.DMA((n_ep, CHUNKS)),
+            pltpu.SemaphoreType.DMA((n_ep, CHUNKS)),
             pltpu.SemaphoreType.DMA((n_ep, CHUNKS)),
             pltpu.SemaphoreType.DMA((n_ep, CHUNKS)),
             pltpu.SemaphoreType.DMA((n_ep, CHUNKS)),

time: 135 us -> 127 us (0.941)
  Pallas kernels: 99.3 us -> 91.6 us
    pallas_call x1, Pallas kernels: 43.1 us -> 35.4 us  [dispatch(): pl.pallas_call(functools.partial(dispatch_kernel, n_ep), out_shape=jax.Sh...]
where the time goes in v3:
time: 127 us
  Pallas kernels  91.6 us (72%)
  matrix products  16.6 us (13%)
  local copies, waits for them, and re-layouts  13.9 us (11%)
  other arithmetic  3.74 us (3%)
    pallas_call x1, Pallas kernels, finish(): pl.pallas_call(functools.partial(finish_kernel, n_ep, n_tp), out_shape=(j...  56.2 us
    pallas_call x1, Pallas kernels, dispatch(): pl.pallas_call(functools.partial(dispatch_kernel, n_ep), out_shape=jax.Sh...  35.4 us
    unnamed x26, local copies, waits for them, and re-layouts  7.61 us
    dot_general x1, matrix products, local(): mine = jnp.dot(pick, source, preferred_element_type=jnp.float32) * factor  3.99 us
    dot_general x1, matrix products, local(): lax.dot_general(flat_scaled, w_down, contract_last, preferred_element_typ...  3.56 us
    dot_general x1, matrix products, local(): lax.dot_general(up_pre, w_up, contract_last, preferred_element_type=jnp.f...  3.52 us
    slice x1, local copies, waits for them, and re-layouts, local(): flat_scaled = both[1].reshape(buffer_rows, model_width)  3.43 us

profile of v3, /device:TPU:0, one launch (start us, length us, event | category | flops | bytes accessed | tf_op | source)
XLA Modules:
  0.0 126.7 jit_solution(17676445336937179044)
XLA Ops:
  0.6 0.0 copy-start
  0.7 0.8 broadcast_multiply_fusion.1
  1.5 0.8 fusion.20
  2.3 0.2 fusion.10
  2.4 0.2 select_reduce_fusion.1
  2.7 0.1 select_n.66
  2.8 0.1 iota.40
  2.8 0.1 eq.64
  2.9 1.1 copy.27
  4.1 1.3 %convert_bitcast_fusion = (bf16[256,768]{1,0:T(8,128)(2,1)S(1)}, pred[768,256]{0,1:T(32,128)(4,1)S(1)}) fusion(s32[768,256]{0,1:T(8,128)} %copy.27, s32[768]{0:T(1024)S(1)} %iota.40), kind=kLoop, calls=%fused_computation.24 | loop fusion | flops 393216 | bytes 1379328 | tf_op jit(solution)/shard_map/transpose | solution.py:637
  5.3 4.0 %multiply_convert_fusion = bf16[768,2048]{1,0:T(8,128)(2,1)} fusion(pred[768,256]{0,1:T(32,128)(4,1)S(1)} %get-tuple-element.28, f32[768]{0:T(1024)S(1)} %select_n.66, bf16[256,2048]{1,0:T(8,128)(2,1)} %param.8, bf16[256,2048]{1,0:T(8,128)(2,1)} %param.9, pred[]{:T(512)S(6)} %eq.67), kind=kOutput, calls=%fused_computation.1 | convolution fusion | flops 808976384 | bytes 5442561 | tf_op jit(solution)/shard_map/dot_general | solution.py:605
  9.3 35.4 %dispatch.1.both_ref = bf16[2,4,192,2048]{3,2,1,0:T(8,128)(2,1)} custom-call(bf16[4,192,2048]{2,1,0:T(8,128)(2,1)} %bitcast.50), custom_call_target="tpu_custom_call" | custom-call | tf_op jit(solution)/shard_map/dispatch/pallas_call | solution.py:116
  44.8 3.4 %fusion.17 = (bf16[1,4,192,2048]{3,2,1,0:T(8,128)(2,1)S(1)}, bf16[1,4,192,2048]{3,2,1,0:T(8,128)(2,1)S(1)}) fusion(bf16[2,4,192,2048]{3,2,1,0:T(8,128)(2,1)} %dispatch.1.both_ref), kind=kLoop, calls=%fused_computation.41 | loop fusion | bytes 12582912 | tf_op jit(solution)/shard_map/slice | solution.py:609
  48.2 0.0 copy-done
  48.2 0.0 copy-start.5
  48.2 1.8 %fusion.2 = f32[768,512]{1,0:T(8,128)S(1)} fusion(bf16[768,2048]{1,0:T(8,128)(2,1)S(1)} %bitcast.51, bf16[1,2048,512]{2,1,0:T(8,128)(2,1)S(1)} %copy-done), kind=kOutput, calls=%fused_computation.4 | convolution fusion | flops 1610612736 | bytes 6815744 | tf_op jit(solution)/shard_map/dot_general | solution.py:617
  50.0 0.0 copy-done.5
  50.0 0.0 copy-start.9
  50.0 1.8 %fusion.5 = f32[768,512]{1,0:T(8,128)S(1)} fusion(bf16[768,2048]{1,0:T(8,128)(2,1)S(1)} %bitcast.52, bf16[1,2048,512]{2,1,0:T(8,128)(2,1)S(1)} %copy-done.5), kind=kOutput, calls=%fused_computation.7 | convolution fusion | flops 1610612736 | bytes 6815744 | tf_op jit(solution)/shard_map/dot_general | solution.py:618
  51.8 0.0 copy-done.9
  51.8 3.6 %multiply_reduce_fusion = (f32[768]{0:T(1024)S(1)}, bf16[768,512]{1,0:T(8,128)(2,1)}, bf16[768,512]{1,0:T(8,128)(2,1)S(1)}, bf16[768,512]{1,0:T(8,128)(2,1)}) fusion(f32[768,512]{1,0:T(8,128)S(1)} %fusion.5, f32[768,512]{1,0:T(8,128)S(1)} %fusion.2, bf16[768,2048]{1,0:T(8,128)(2,1)S(1)} %bitcast.49, bf16[1,512,2048]{2,1,0:T(8,128)(2,1)S(1)} %copy-done.9), kind=kOutput, calls=%fused_computation.11 | convolution fusion | flops 1617689856 | bytes 10750976 | tf_op jit(solution)/shard_map/dot_general | solution.py:623
  55.4 0.1 reshape.128
  55.5 0.0 copy-start.1
  55.5 0.0 copy-start.6
  55.5 1.8 %fusion = f32[768,2048]{1,0:T(8,128)S(1)} fusion(bf16[768,512]{1,0:T(8,128)(2,1)S(1)} %get-tuple-element.33.gate_ref, bf16[1,2048,512]{2,1,0:T(8,128)(2,1)S(1)} %copy-done), kind=kOutput, calls=%fused_computation.2 | convolution fusion | flops 1610612736 | bytes 9175040 | tf_op jit(solution)/shard_map/dot_general | solution.py:629
  57.3 0.0 copy-done.1
  57.4 0.0 copy-done.6
  57.4 0.0 copy-start.2
  57.4 3.5 %add_convert_fusion = bf16[768,2048]{1,0:T(8,128)(2,1)} fusion(f32[768,2048]{1,0:T(8,128)S(1)} %fusion, bf16[768,512]{1,0:T(8,128)(2,1)S(1)} %copy-done.1, bf16[1,2048,512]{2,1,0:T(8,128)(2,1)S(1)} %copy-done.6), kind=kOutput, calls=%fused_computation | convolution fusion | flops 1613758464 | bytes 12320768 | tf_op jit(solution)/shard_map/dot_general | solution.py:632
  60.9 0.0 copy-done.2
  60.9 0.0 copy-start.7
  60.9 0.0 copy-start.8
  60.9 56.2 %finish.1 = (bf16[256,2048]{1,0:T(8,128)(2,1)S(1)}, bf16[2048,512]{1,0:T(8,128)(2,1)S(1)}, bf16[2048,512]{1,0:T(8,128)(2,1)}, bf16[512,2048]{1,0:T(8,128)(2,1)},...) custom-call(bf16[2,4,192,2048]{3,2,1,0:T(8,128)(2,1)} %dispatch.1.both_ref, ...), custom_call_target="tpu_custom_call" | custom-call | tf_op jit(solution)/shard_map/finish/pallas_call | solution.py:523
  117.1 0.2 select_reduce_fusion
  117.3 0.0 copy-done.7
  117.3 0.0 copy-done.8
  117.3 0.6 broadcast_multiply_fusion
  117.9 0.6 multiply_reduce_fusion.1
  118.5 0.6 fusion.18
  119.1 1.0 copy.49
  120.1 0.0 copy-start.4
  120.1 1.3 %copy.50 = bf16[1,2048,512]{2,1,0:T(8,128)(2,1)} copy(bf16[1,2048,512]{2,1,0:T(8,128)(2,1)S(1)} %bitcast.44) | data formatting | bytes 4194304
  121.4 1.0 copy-done.4
  122.4 0.0 copy-start.3
  122.4 1.3 %copy.51 = bf16[1,2048,512]{2,1,0:T(8,128)(2,1)} copy(bf16[1,2048,512]{2,1,0:T(8,128)(2,1)S(1)} %bitcast.54) | data formatting | bytes 4194304
  123.7 1.0 copy-done.3
  124.8 1.3 %copy.52 = bf16[1,512,2048]{2,1,0:T(8,128)(2,1)} copy(bf16[1,512,2048]{2,1,0:T(8,128)(2,1)S(1)} %bitcast.53) | data formatting | bytes 4194304
  126.1 0.6 copy.53
  (9 shorter events, 0.1 us)
Async XLA Ops:
  0.6 47.6 %copy-start = (bf16[1,2048,512]{2,1,0:T(8,128)(2,1)S(1)}, bf16[1,2048,512]{2,1,0:T(8,128)(2,1)}, u32[]{:S(2)}) copy-start(bf16[1,2048,512]{2,1,0:T(8,128)(2,1)} %param.13) | copy-start | bytes 6291460
  48.2 1.8 %copy-start.5 = (bf16[1,2048,512]{2,1,0:T(8,128)(2,1)S(1)}, bf16[1,2048,512]{2,1,0:T(8,128)(2,1)}, u32[]{:S(2)}) copy-start(bf16[1,2048,512]{2,1,0:T(8,128)(2,1)} %param.14) | copy-start | bytes 6291460
  50.0 1.8 %copy-start.9 = (bf16[1,512,2048]{2,1,0:T(8,128)(2,1)S(1)}, bf16[1,512,2048]{2,1,0:T(8,128)(2,1)}, u32[]{:S(2)}) copy-start(bf16[1,512,2048]{2,1,0:T(8,128)(2,1)} %param.15) | copy-start | bytes 6291460
  55.5 1.9 %copy-start.1 = (bf16[768,512]{1,0:T(8,128)(2,1)S(1)}, bf16[768,512]{1,0:T(8,128)(2,1)}, u32[]{:S(2)}) copy-start(bf16[768,512]{1,0:T(8,128)(2,1)} %get-tuple-element.34.up_ref) | copy-start | bytes 2359300
  55.5 1.9 %copy-start.6 = (bf16[1,2048,512]{2,1,0:T(8,128)(2,1)S(1)}, bf16[1,2048,512]{2,1,0:T(8,128)(2,1)}, u32[]{:S(2)}) copy-start(bf16[1,2048,512]{2,1,0:T(8,128)(2,1)} %param.14) | copy-start | bytes 6291460
  57.4 3.5 %copy-start.2 = (bf16[768,512]{1,0:T(8,128)(2,1)S(1)}, bf16[768,512]{1,0:T(8,128)(2,1)}, u32[]{:S(2)}) copy-start(bf16[768,512]{1,0:T(8,128)(2,1)} %get-tuple-element.30.hid_ref) | copy-start | bytes 2359300
  60.9 56.4 %copy-start.7 = (f32[256,2]{0,1:T(2,128)S(1)}, f32[256,2]{0,1:T(2,128)}, u32[]{:S(2)}) copy-start(f32[256,2]{0,1:T(2,128)} %param.11) | copy-start | bytes 6148
  60.9 56.4 %copy-start.8 = (f32[256]{0:T(256)S(1)}, f32[256]{0:T(256)}, u32[]{:S(2)}) copy-start(f32[256]{0:T(256)} %param.10) | copy-start | bytes 3076
  120.1 2.3 %copy-start.4 = (bf16[2048,512]{1,0:T(8,128)(2,1)S(1)}, bf16[2048,512]{1,0:T(8,128)(2,1)}, u32[]{:S(2)}) copy-start(bf16[2048,512]{1,0:T(8,128)(2,1)} %get-tuple-element.19) | copy-start | bytes 6291460
  122.4 2.3 %copy-start.3 = (bf16[512,2048]{1,0:T(8,128)(2,1)S(1)}, bf16[512,2048]{1,0:T(8,128)(2,1)}, u32[]{:S(2)}) copy-start(bf16[512,2048]{1,0:T(8,128)(2,1)} %get-tuple-element.20) | copy-start | bytes 6291460
